TPU v7x, 32 devices: a whole 2x2x4 slice. The times are simulated.
32 devices in a mesh: ep: 8 (over z, x), tp: 4 (over y, core).
Axes of the slice: x: 2, y: 2, z: 4, core: 2. Of those that a mesh axis runs over, the one named last changes fastest.
Arguments:
- tokens: bfloat16 [512, 4096], P('ep'), may hold values from -6 to 6
- state_in: float32 [512, 4096], P('ep', 'tp'), may hold values from -6 to 6
- conv_in: bfloat16 [512, 3, 4096], P('ep', None, 'tp'), may hold values from -6 to 6
- mix_gain: bfloat16 [4096], replicated, may hold values from 0.099609375 to 1.8984375
- rnn_weight: bfloat16 [4096, 4096], P('ep', 'tp'), may hold values from -0.09375 to 0.09375
- gate_weight: bfloat16 [4096, 4096], P('ep', 'tp'), may hold values from -0.09375 to 0.09375
- conv_weight: bfloat16 [4, 4096], P(None, 'tp'), may hold values from -3 to 3
- rate_weight: bfloat16 [16, 256, 256], P('tp'), may hold values from -0.375 to 0.375
- input_weight: bfloat16 [16, 256, 256], P('tp'), may hold values from -0.375 to 0.375
- rate_param: float32 [4096], P('tp'), may hold values from 1 to 6
- out_weight: bfloat16 [4096, 4096], P('tp'), may hold values from -0.09375 to 0.09375
- moe_gain: bfloat16 [4096], replicated, may hold values from 0.099609375 to 1.8984375
- expert_gate: bfloat16 [8, 4096, 2048], P('ep', None, 'tp'), may hold values from -0.09375 to 0.09375
- expert_up: bfloat16 [8, 4096, 2048], P('ep', None, 'tp'), may hold values from -0.09375 to 0.09375
- expert_down: bfloat16 [8, 2048, 4096], P('ep', 'tp'), may hold values from -0.125 to 0.125
- routes: int32 [512, 2], P('ep'), may hold values from 0 to 7, all different within a row; in each aligned block of 64 rows (0 to 63, 64 to 127, ...) at most 32 rows name the same one
- route_prob: float32 [512, 2], P('ep'), may hold values from 0.1 to 1
Outputs:
- layer_out: bfloat16 [512, 4096], P('ep', 'tp')
- state_out: float32 [512, 4096], P('ep', 'tp')
- conv_out: bfloat16 [512, 3, 4096], P('ep', None, 'tp')
Inputs may be any that keep to these rules, and one draw needn't show every extreme that they name: `routes`: the 2 experts of a sequence differ. Among the rows of one index of ep no expert is named more than 32 times, and in every draw some expert is named exactly 32 times there.
All inputs are finite; a program needn't handle non-finite values.
Results may differ from a plain program's by a relative error of at most 0.014.
Values may be sent and summed in bfloat16 or wider, within the bound.
A program may use at most 64 MiB of HBM per device.

v0:
```python
import functools

import jax
import jax.numpy as jnp
from jax import lax
from jax.experimental import pallas as pl
from jax.experimental.pallas import tpu as pltpu
from jax.sharding import PartitionSpec as P

MESH = pl.DeviceIdType.MESH
F32 = jnp.float32
BF16 = jnp.bfloat16


def dot(a, b):
    return jnp.dot(a, b, preferred_element_type=F32)


def remote(src, dst, send, recv, where):
    return pltpu.make_async_remote_copy(
        src_ref=src, dst_ref=dst, send_sem=send, recv_sem=recv, device_id=where, device_id_type=MESH
    )


def kernel(
    n, p, nx, cap,
    tokens, state_in, conv_in, mix_gain_in, moe_gain_in, conv_w, rate_param, routes, prob,
    rnn_h, gate_h, rate_h, input_h, out_h, eg_h, eu_h, ed_h,
    layer_out, state_out, moved_out,
    wr, wg, wrate, winput, wout, weg, weu, wed,
    mix_gain, moe_gain, normed, cols, part, bx, zsend, rbuf, gated,
    op_p, op_o, op_r, hs, hr, mixed,
    sd, rows, xn, hid, e_p, e_o, e_r, es, er, outb, ret,
    wsem, sa, ra, sa2, ra2, sb, rb, sbz, rbz, sd1, rd1, sd2, rd2, sc1, rc1, sc2, rc2, sc3, rc3,
    se1, re1, se2, re2, se3, re3,
):
    e = lax.axis_index("ep")
    t = lax.axis_index("tp")
    core = lax.rem(t, 2)
    y = t // 2
    q = t + 1 - 2 * core
    ys = p // 2
    nz = n // nx
    z = e // nx
    x = lax.rem(e, nx)
    far_first = sorted(range(nz), key=lambda dz: -min(dz, nz - dz))

    def up(d):
        return lax.rem(z + d // nx, nz) * nx + lax.rem(x + d % nx, nx)

    def down_of(d):
        return lax.rem(z - d // nx + nz, nz) * nx + lax.rem(x - d % nx + nx, nx)

    rows_g, width = tokens.shape
    depth = width // n
    chans = rnn_h.shape[1]
    share = width // p
    slots = n * cap

    loads = [
        pltpu.make_async_copy(a, b, wsem.at[i])
        for i, (a, b) in enumerate(
            [(rnn_h, wr), (gate_h, wg), (rate_h, wrate), (input_h, winput), (out_h, wout),
             (eg_h.at[0], weg), (eu_h.at[0], weu), (ed_h.at[0], wed)]
        )
    ]
    for load in loads[:4]:
        load.start()

    barrier = pltpu.get_barrier_semaphore()

    @pl.loop(1, n)
    def _(d):
        pl.semaphore_signal(barrier, inc=1, device_id={"ep": lax.rem(e + d, n)}, device_id_type=MESH)

    @pl.loop(1, p)
    def _(d):
        pl.semaphore_signal(barrier, inc=1, device_id={"tp": lax.rem(t + d, p)}, device_id_type=MESH)

    for j in range(width // 128):
        cs = slice(j * 128, (j + 1) * 128)
        mix_gain[:, cs] = mix_gain_in[j:j + 1, :].astype(F32)
        moe_gain[:, cs] = moe_gain_in[j:j + 1, :].astype(F32)

    ssq = jnp.zeros((rows_g, 1), F32)
    for j in range(n):
        v = tokens[:, j * depth:(j + 1) * depth].astype(F32)
        ssq = ssq + jnp.sum(v * v, axis=1, keepdims=True)
    scale = lax.rsqrt(ssq / width + 1e-06)
    for j in range(n):
        cs = slice(j * depth, (j + 1) * depth)
        normed[j] = (tokens[:, cs].astype(F32) * scale * mix_gain[:, cs]).astype(BF16)

    pl.semaphore_wait(barrier, n + p - 2)

    half = pl.ds(pl.multiple_of(core * (rows_g // 2), rows_g // 2), rows_g // 2)

    def copy_a(d):
        peer = up(d)
        return remote(normed.at[peer, half], cols.at[e, half], sa.at[d], ra.at[d], {"ep": peer})

    def copy_a2(d):
        src = down_of(d)
        return remote(cols.at[src, half], cols.at[src, half], sa2.at[d], ra2.at[d], {"tp": q})

    away_first = list(range(1, nz)) + [0]
    for dz in away_first:
        for dx in range(nx):
            if dz + dx:
                copy_a(dz * nx + dx).start()
    cols[e] = normed[e]

    ids = routes[...]
    sub_e = lax.broadcasted_iota(jnp.int32, (n, rows_g), 0)
    named = [(ids[k:k + 1, :] == sub_e).astype(F32) for k in range(ids.shape[0])]
    member = functools.reduce(lambda a, b: a + b, named)
    earlier = (
        lax.broadcasted_iota(jnp.int32, (rows_g, rows_g), 0)
        < lax.broadcasted_iota(jnp.int32, (rows_g, rows_g), 1)
    ).astype(F32)
    before = dot(member.astype(BF16), earlier.astype(BF16))
    sub_s = lax.broadcasted_iota(jnp.int32, (slots, rows_g), 0).astype(F32)
    total_prob = jnp.sum(prob[...], axis=0, keepdims=True)
    dispatch = jnp.zeros((slots, rows_g), F32)
    comb = jnp.zeros((slots, rows_g), F32)
    for k in range(ids.shape[0]):
        slot = jnp.sum(before * named[k], axis=0, keepdims=True)
        target = ids[k:k + 1, :].astype(F32) * cap + slot
        hit = (sub_s == target).astype(F32)
        dispatch = dispatch + hit
        comb = comb + hit * (prob[k:k + 1, :] / total_prob)
    dispatch = dispatch.astype(BF16)
    comb_hi = comb.astype(BF16)
    comb_lo = (comb - comb_hi.astype(F32)).astype(BF16)

    loads[0].wait()
    loads[1].wait()
    for load in loads[4:]:
        load.start()

    def copy_b(dz, dx):
        zs = lax.rem(z - dz + nz, nz)
        peer = z * nx + lax.rem(x - dx + nx, nx)
        return remote(part.at[dz, dx], bx.at[dz, dx], sb.at[dz, dx], rb.at[dz, dx], {"ep": peer})

    def copy_bz(dz):
        peer = lax.rem(z - dz + nz, nz) * nx + x
        return remote(zsend.at[dz], rbuf.at[dz], sbz.at[dz], rbz.at[dz], {"ep": peer})

    def pass_on(dz):
        for lo in (0, chans):
            cs = slice(lo, lo + chans)
            if lo == 0:
                for dx in range(1, nx):
                    copy_b(dz, dx).wait_recv()
            acc = part[dz, 0, :, cs].astype(F32)
            for dx in range(1, nx):
                acc = acc + bx[dz, dx, :, cs].astype(F32)
            if dz:
                zsend[dz, :, cs] = acc.astype(BF16)
            else:
                rbuf[0, :, cs] = acc.astype(BF16)
        if dz:
            copy_bz(dz).start()

    for k, dz in enumerate(away_first):
        for dx in range(nx):
            d = dz * nx + dx
            if d:
                copy_a(d).wait_recv()
                copy_a2(d).start()
        for dx in list(range(1, nx)) + [0]:
            d = dz * nx + dx
            if d:
                copy_a2(d).wait_recv()
            src = down_of(d)
            part[dz, dx, :, :chans] = dot(cols[src], wr[...]).astype(BF16)
            part[dz, dx, :, chans:] = dot(cols[src], wg[...]).astype(BF16)
            if dx:
                copy_b(dz, dx).start()
        if k:
            pass_on(away_first[k - 1])
    pass_on(0)
    for dz in range(1, nz):
        copy_bz(dz).wait_recv()

    loads[2].wait()
    loads[3].wait()
    bw = rate_h.shape[1]
    for b in range(rate_h.shape[0]):
        cs = slice(b * bw, (b + 1) * bw)
        cy = slice(chans + b * bw, chans + (b + 1) * bw)
        proj_x = rbuf[0, :, cs].astype(F32)
        proj_y = rbuf[0, :, cy].astype(F32)
        for j in range(1, nz):
            proj_x = proj_x + rbuf[j, :, cs].astype(F32)
            proj_y = proj_y + rbuf[j, :, cy].astype(F32)
        moved = proj_x.astype(BF16)
        moved_out[:, cs] = moved
        taps = conv_w[:, cs].astype(F32)
        hist = conv_in[0, :, cs].astype(F32) * taps[0:1]
        for i in range(1, 3):
            hist = hist + conv_in[i, :, cs].astype(F32) * taps[i:i + 1]
        conv = (hist + moved.astype(F32) * taps[3:4]).astype(BF16)
        rate = jax.nn.sigmoid(dot(conv, wrate[b]))
        in_gate = jax.nn.sigmoid(dot(conv, winput[b]))
        log_decay = -8.0 * rate * jnp.log1p(jnp.exp(-rate_param[:, cs]))
        th = jnp.tanh(log_decay)
        rest = -2.0 * th / (1.0 - th)
        state = jnp.exp(log_decay) * state_in[:, cs] + jnp.sqrt(rest) * in_gate * conv.astype(F32)
        state_out[:, cs] = state
        gated[:, cs] = (state * jax.nn.gelu(proj_y, approximate=True)).astype(BF16)

    def block(i):
        return pl.ds(pl.multiple_of(i * share, share), share)

    loads[4].wait()

    def copy_d1(yy):
        return remote(op_p.at[yy], op_r.at[yy], sd1.at[yy], rd1.at[yy], {"tp": q})

    def copy_d2(dy):
        ty = lax.rem(y + dy, ys)
        return remote(hs.at[ty], hr.at[y], sd2.at[dy], rd2.at[dy], {"tp": ty * 2 + core})

    for dy in range(ys):
        yy = lax.rem(y + dy + 1, ys)
        op_p[yy] = dot(gated[...], wout[:, block(yy * 2 + 1 - core)]).astype(BF16)
        copy_d1(yy).start()
    for dy in range(ys):
        yy = lax.rem(y + dy + 1, ys)
        op_o[yy] = dot(gated[...], wout[:, block(yy * 2 + core)])
    for dy in range(1, ys):
        ty = lax.rem(y + dy, ys)
        copy_d1(ty).wait_recv()
        hs[ty] = (op_o[ty] + op_r[ty].astype(F32)).astype(BF16)
        copy_d2(dy).start()
    copy_d1(y).wait_recv()
    total = tokens[:, block(t)].astype(F32) + op_o[y] + op_r[y].astype(F32)
    for dy in range(1, ys):
        copy_d2(dy).wait_recv()
        total = total + hr[lax.rem(y - dy + ys, ys)].astype(F32)
    mixed[...] = total

    sent = dot(dispatch, mixed[...].astype(BF16))
    sd[...] = sent.reshape(n, cap, share).astype(BF16)

    def copy_c1(d):
        peer = up(d)
        return remote(sd.at[peer], rows.at[t, e], sc1.at[d], rc1.at[d], {"ep": peer})

    def copy_c2(dy, d):
        src = down_of(d)
        to = lax.rem(y + dy, ys) * 2 + core
        return remote(rows.at[t, src], rows.at[t, src], sc2.at[dy, d], rc2.at[dy, d], {"tp": to})

    def copy_c3(dy, d):
        src = down_of(d)
        held = lax.rem(y - dy + ys, ys) * 2 + core
        return remote(rows.at[held, src], rows.at[held, src], sc3.at[dy, d], rc3.at[dy, d], {"tp": q})

    order = [dz * nx + dx for dz in far_first for dx in range(nx) if dz + dx]
    for d in order:
        copy_c1(d).start()

    rows[t, e] = sd[e]

    def spread(d):
        for dy in range(1, ys):
            copy_c2(dy, d).start()
        copy_c3(0, d).start()

    def relay(d):
        for dy in range(1, ys):
            copy_c2(dy, d).wait_recv()
            copy_c3(dy, d).start()

    near = order[::-1]
    spread(0)
    for i, d in enumerate(near):
        copy_c1(d).wait_recv()
        spread(d)
        if i >= 1:
            relay(([0] + near)[i - 1])
    for d in ([0] + near)[len(near) - 1:]:
        relay(d)
    for d in range(n):
        for dy in range(ys):
            copy_c3(dy, d).wait_recv()

    gs = min(n, max(1, 64 // cap))
    span = gs * cap

    @pl.loop(0, n // gs)
    def _(g):
        def piece(i):
            return rows[i, pl.ds(g * gs, gs)].astype(F32).reshape(span, share)

        acc = jnp.zeros((span, 1), F32)
        for i in range(p):
            v = piece(i)
            acc = acc + jnp.sum(v * v, axis=1, keepdims=True)
        sc = lax.rsqrt(acc / width + 1e-06)
        for i in range(p):
            cs = slice(i * share, (i + 1) * share)
            xn[pl.ds(pl.multiple_of(g * span, span), span), cs] = (
                piece(i) * sc * moe_gain[:, cs]
            ).astype(BF16)

    loads[5].wait()
    loads[6].wait()
    hidden = hid.shape[1]
    fc = min(256, hidden)

    @pl.loop(0, hidden // fc)
    def _(c):
        cs = pl.ds(pl.multiple_of(c * fc, fc), fc)
        gate_part = dot(xn[...], weg[:, cs])
        up_part = dot(xn[...], weu[:, cs])
        hid[:, cs] = (jax.nn.silu(gate_part) * up_part).astype(BF16)

    loads[7].wait()

    def copy_e1(yy):
        return remote(e_p.at[yy], e_r.at[yy], se1.at[yy], re1.at[yy], {"tp": q})

    def copy_e2(dy, dz):
        ty = lax.rem(y + dy, ys)
        zc = lax.rem(z + dz, nz)
        return remote(
            es.at[ty, zc], er.at[y, zc], se2.at[dy, dz], re2.at[dy, dz], {"tp": ty * 2 + core}
        )

    def copy_e3(d):
        peer = up(d)
        return remote(outb.at[peer], ret.at[e], se3.at[d], re3.at[d], {"ep": peer})

    nc = min(256, share)
    chunk = nx * cap

    def down(yy, parity, dst):
        @pl.loop(0, share // nc)
        def _(c):
            at = pl.ds(pl.multiple_of((yy * 2 + parity) * share + c * nc, nc), nc)
            value = dot(hid[...], wed[:, at]).reshape(nz, chunk, nc)
            dst[yy, :, :, pl.ds(pl.multiple_of(c * nc, nc), nc)] = value.astype(dst.dtype)

    for dy in list(range(1, ys)) + [0]:
        ty = lax.rem(y + dy, ys)
        down(ty, 1 - core, e_p)
        copy_e1(ty).start()
        down(ty, core, e_o)
        copy_e1(ty).wait_recv()
        if dy:
            for dz in far_first:
                zc = lax.rem(z + dz, nz)
                es[ty, zc] = (e_o[ty, zc] + e_r[ty, zc].astype(F32)).astype(BF16)
                copy_e2(dy, dz).start()
    for dz in far_first:
        zc = lax.rem(z + dz, nz)
        result = e_o[y, zc] + e_r[y, zc].astype(F32)
        for dy in range(1, ys):
            copy_e2(dy, dz).wait_recv()
            result = result + er[lax.rem(y - dy + ys, ys), zc].astype(F32)
        outb[pl.ds(zc * nx, nx)] = result.reshape(nx, cap, share).astype(BF16)
        for dx in range(nx):
            if dz + dx:
                copy_e3(dz * nx + dx).start()

    ret[e] = outb[e]
    for d in order:
        copy_e3(d).wait_recv()

    back = ret[...].astype(F32).reshape(slots, share).astype(BF16)

    def combine(weights):
        return lax.dot_general(weights, back, (((0,), (0,)), ((), ())), preferred_element_type=F32)

    layer_out[...] = (mixed[...] + combine(comb_hi) + combine(comb_lo)).astype(BF16)

    @pl.loop(1, n)
    def _(d):
        copy_a(d).wait_send()
        copy_a2(d).wait_send()
        copy_c1(d).wait_send()
        copy_e3(d).wait_send()

    @pl.loop(0, n)
    def _(d):
        for dy in range(1, ys):
            copy_c2(dy, d).wait_send()
        for dy in range(ys):
            copy_c3(dy, d).wait_send()

    for dy in range(ys):
        copy_d1(dy).wait_send()
        copy_e1(dy).wait_send()
    for dy in range(1, ys):
        copy_d2(dy).wait_send()
        for dz in range(nz):
            copy_e2(dy, dz).wait_send()
    for dz in range(nz):
        for dx in range(1, nx):
            copy_b(dz, dx).wait_send()
        if dz:
            copy_bz(dz).wait_send()


def finish(layer_in, state_in, moved, conv_in, layer_out, state_out, conv_out):
    layer_out[...] = layer_in[...]
    state_out[...] = state_in[...]
    kept = conv_in.shape[0] - 1
    for i in range(kept):
        conv_out[i] = conv_in[i + 1]
    conv_out[kept] = moved[...]


def shards(
    n, p,
    tokens, state_in, conv_in, mix_gain, rnn_weight, gate_weight, conv_weight, rate_weight,
    input_weight, rate_param, out_weight, moe_gain, expert_gate, expert_up, expert_down, routes, route_prob,
):
    g, width = tokens.shape
    depth, chans = rnn_weight.shape
    share = width // p
    cap = max(2, 2 * g * routes.shape[1] // n)
    slots = n * cap
    hidden = expert_gate.shape[2]
    ys = p // 2
    nx = 1 << ((n.bit_length() - 1) // 2)
    nx = nx if n % nx == 0 else 1
    nz = n // nx
    conv_t = jnp.transpose(conv_in, (1, 0, 2))
    vm = pl.BlockSpec(memory_space=pltpu.VMEM)
    hb = pl.BlockSpec(memory_space=pl.ANY)
    dma = pltpu.SemaphoreType.DMA
    V = pltpu.VMEM
    scratch = [
        V((depth, chans), BF16), V((depth, chans), BF16),
        V(rate_weight.shape, BF16), V(input_weight.shape, BF16), V(out_weight.shape, BF16),
        V(expert_gate.shape[1:], BF16), V(expert_up.shape[1:], BF16), V(expert_down.shape[1:], BF16),
        V((1, width), F32), V((1, width), F32),
        V((n, g, depth), BF16), V((n, g, depth), BF16),
        V((nz, nx, g, 2 * chans), BF16), V((nz, nx, g, 2 * chans), BF16),
        V((nz, g, 2 * chans), BF16), V((nz, g, 2 * chans), BF16),
        V((g, chans), BF16),
        V((ys, g, share), BF16), V((ys, g, share), F32), V((ys, g, share), BF16),
        V((ys, g, share), BF16), V((ys, g, share), BF16), V((g, share), F32),
        V((n, cap, share), BF16), V((p, n, cap, share), BF16), V((slots, width), BF16), V((slots, hidden), BF16),
        V((ys, nz, nx * cap, share), BF16), V((ys, nz, nx * cap, share), F32), V((ys, nz, nx * cap, share), BF16),
        V((ys, nz, nx * cap, share), BF16), V((ys, nz, nx * cap, share), BF16),
        V((n, cap, share), BF16), V((n, cap, share), BF16),
        dma((8,)),
        dma((n,)), dma((n,)), dma((n,)), dma((n,)), dma((nz, nx)), dma((nz, nx)), dma((nz,)), dma((nz,)),
        dma((ys,)), dma((ys,)), dma((ys,)), dma((ys,)),
        dma((n,)), dma((n,)), dma((ys, n)), dma((ys, n)), dma((ys, n)), dma((ys, n)),
        dma((ys,)), dma((ys,)), dma((ys, nz)), dma((ys, nz)), dma((n,)), dma((n,)),
    ]
    layer, state, moved = pl.pallas_call(
        functools.partial(kernel, n, p, nx, cap),
        out_shape=(
            jax.ShapeDtypeStruct((g, share), BF16),
            jax.ShapeDtypeStruct((g, chans), F32),
            jax.ShapeDtypeStruct((g, chans), BF16),
        ),
        in_specs=[vm] * 9 + [hb] * 8,
        out_specs=(vm, vm, vm),
        scratch_shapes=scratch,
        compiler_params=pltpu.CompilerParams(
            collective_id=0, has_side_effects=True, vmem_limit_bytes=60 * 1024 * 1024
        ),
    )(
        tokens, state_in, conv_t, mix_gain.reshape(-1, 128), moe_gain.reshape(-1, 128),
        conv_weight, rate_param[None], routes.T, route_prob.T,
        rnn_weight, gate_weight, rate_weight, input_weight, out_weight, expert_gate, expert_up, expert_down,
    )
    layer_out, state_out, conv_out = pl.pallas_call(
        finish,
        out_shape=(
            jax.ShapeDtypeStruct(layer.shape, layer.dtype),
            jax.ShapeDtypeStruct(state.shape, state.dtype),
            jax.ShapeDtypeStruct(conv_t.shape, conv_t.dtype),
        ),
        in_specs=[vm] * 4,
        out_specs=(vm, vm, vm),
    )(layer, state, moved, conv_t)
    return (layer_out, state_out, jnp.transpose(conv_out, (1, 0, 2)))


def solution(mesh):
    in_specs = (
        P("ep", None),
        P("ep", "tp"),
        P("ep", None, "tp"),
        P(),
        P("ep", "tp"),
        P("ep", "tp"),
        P(None, "tp"),
        P("tp", None, None),
        P("tp", None, None),
        P("tp"),
        P("tp", None),
        P(),
        P("ep", None, "tp"),
        P("ep", None, "tp"),
        P("ep", "tp", None),
        P("ep", None),
        P("ep", None),
    )
    out_specs = (P("ep", "tp"), P("ep", "tp"), P("ep", None, "tp"))
    body = functools.partial(shards, mesh.shape["ep"], mesh.shape["tp"])
    return jax.shard_map(body, mesh=mesh, in_specs=in_specs, out_specs=out_specs, check_vma=False)
```

profile of v0, /device:TPU:0, one launch (start us, length us, event | category | flops | bytes accessed | tf_op | source)
XLA Modules:
  0.0 104.5 jit_solution(13617468371669196236)
XLA Ops:
  0.6 101.8 %shard_map.184 = (bf16[64,1024]{1,0:T(8,128)(2,1)}, f32[64,1024]{1,0:T(8,128)}, bf16[64,1024]{1,0:T(8,128)(2,1)}) custom-call(bf16[64,4096]{1,0:T(8,128)(2,1)} %tokens.1, f32[64,1024]{1,0:T(8,128)} %state_in.1, bf16[3,64,1024]{2,1,0:T(8,128)(2,1)} %bitcast.7, bf16[32,128]{1,0:T(8,128)(2,1)} %bitcast.9, bf16[32,128]{1,0:T(8,128)(2,1)} %bitcast.10, ...), custom_call_target="tpu_custom_call" | custom-call | tf_op jit(solution)/shard_map/pallas_call | solution.py:459
  102.4 2.1 %shard_map.185 = (bf16[64,1024]{1,0:T(8,128)(2,1)}, f32[64,1024]{1,0:T(8,128)}, bf16[3,64,1024]{2,1,0:T(8,128)(2,1)}) custom-call(bf16[64,1024]{1,0:T(8,128)(2,1)} %get-tuple-element.9.layer_in, f32[64,1024]{1,0:T(8,128)} %get-tuple-element.10.state_in, bf16[64,1024]{1,0:T(8,128)(2,1)} %get-tuple-element.11.moved, bf16[3,64,1024]{2,1,0:T(8,128)(2,1)} %bitcast.8), custom_call_target="tpu_custom_call" | custom-call | tf_op jit(solution)/shard_map/pallas_call | solution.py:477
where the time goes:
time: 105 us; the launch traced here: 104 us
  Pallas kernels  104 us (99%)
    pallas_call x1, Pallas kernels, shards(): pl.pallas_call(functools.partial(kernel, n, p, nx, cap), out_shape=(jax.S...  102 us

commit v1 on v0

--- a/solution.py
+++ b/solution.py
@@ -28,10 +28,10 @@
     rnn_h, gate_h, rate_h, input_h, out_h, eg_h, eu_h, ed_h,
     layer_out, state_out, moved_out,
     wr, wg, wrate, winput, wout, weg, weu, wed,
-    mix_gain, moe_gain, normed, cols, part, bx, zsend, rbuf, gated,
+    mix_gain, moe_gain, normed, cols, part, bx, zsend, rz, gated, oacc,
     op_p, op_o, op_r, hs, hr, mixed,
     sd, rows, xn, hid, e_p, e_o, e_r, es, er, outb, ret,
-    wsem, sa, ra, sa2, ra2, sb, rb, sbz, rbz, sd1, rd1, sd2, rd2, sc1, rc1, sc2, rc2, sc3, rc3,
+    wsem, sa, ra, sa2, ra2, sb, rb, sz, rzs, sd1, rd1, sd2, rd2, sc1, rc1, sc2, rc2, sc3, rc3,
     se1, re1, se2, re2, se3, re3,
 ):
     e = lax.axis_index("ep")
@@ -91,23 +91,47 @@
         cs = slice(j * depth, (j + 1) * depth)
         normed[j] = (tokens[:, cs].astype(F32) * scale * mix_gain[:, cs]).astype(BF16)
 
+    @pl.when(z == 0)
+    def _():
+        rz[0] = jnp.zeros(rz.shape[1:], BF16)
+
+    @pl.when(z == nz - 1)
+    def _():
+        rz[1] = jnp.zeros(rz.shape[1:], BF16)
+
     pl.semaphore_wait(barrier, n + p - 2)
 
+
     half = pl.ds(pl.multiple_of(core * (rows_g // 2), rows_g // 2), rows_g // 2)
-
-    def copy_a(d):
-        peer = up(d)
-        return remote(normed.at[peer, half], cols.at[e, half], sa.at[d], ra.at[d], {"ep": peer})
-
-    def copy_a2(d):
-        src = down_of(d)
-        return remote(cols.at[src, half], cols.at[src, half], sa2.at[d], ra2.at[d], {"tp": q})
-
-    away_first = list(range(1, nz)) + [0]
-    for dz in away_first:
+    nc, bw = rate_h.shape[0], rate_h.shape[1]
+    high = (2 * z) // nz
+    folded = z + high * (nz - 1 - 2 * z)
+
+    def far(j):
+        plane = nz - 1 - j
+        plane = plane - (folded >= plane).astype(jnp.int32)
+        return plane + high * (nz - 1 - 2 * plane)
+
+    def beside(dx):
+        return lax.rem(x + dx, nx)
+
+    def copy_a(peer):
+        return remote(normed.at[peer, half], cols.at[e, half], sa.at[peer], ra.at[e], {"ep": peer})
+
+    def landed_a(src):
+        return remote(normed.at[src, half], cols.at[src, half], sa.at[src], ra.at[src], {"ep": src})
+
+    def copy_a2(src):
+        return remote(cols.at[src, half], cols.at[src, half], sa2.at[src], ra2.at[src], {"tp": q})
+
+    for dx in range(1, nx):
+        copy_a(z * nx + beside(dx)).start()
+
+    @pl.loop(0, nz - 1)
+    def _(j):
         for dx in range(nx):
-            if dz + dx:
-                copy_a(dz * nx + dx).start()
+            copy_a(far(j) * nx + beside(dx)).start()
+
     cols[e] = normed[e]
 
     ids = routes[...]
@@ -138,83 +162,105 @@
     for load in loads[4:]:
         load.start()
 
-    def copy_b(dz, dx):
-        zs = lax.rem(z - dz + nz, nz)
-        peer = z * nx + lax.rem(x - dx + nx, nx)
-        return remote(part.at[dz, dx], bx.at[dz, dx], sb.at[dz, dx], rb.at[dz, dx], {"ep": peer})
-
-    def copy_bz(dz):
-        peer = lax.rem(z - dz + nz, nz) * nx + x
-        return remote(zsend.at[dz], rbuf.at[dz], sbz.at[dz], rbz.at[dz], {"ep": peer})
-
-    def pass_on(dz):
-        for lo in (0, chans):
-            cs = slice(lo, lo + chans)
-            if lo == 0:
-                for dx in range(1, nx):
-                    copy_b(dz, dx).wait_recv()
-            acc = part[dz, 0, :, cs].astype(F32)
-            for dx in range(1, nx):
-                acc = acc + bx[dz, dx, :, cs].astype(F32)
-            if dz:
-                zsend[dz, :, cs] = acc.astype(BF16)
-            else:
-                rbuf[0, :, cs] = acc.astype(BF16)
-        if dz:
-            copy_bz(dz).start()
-
-    for k, dz in enumerate(away_first):
-        for dx in range(nx):
-            d = dz * nx + dx
-            if d:
-                copy_a(d).wait_recv()
-                copy_a2(d).start()
+    def copy_x(plane, dx, c):
+        return remote(
+            part.at[plane, dx, c], bx.at[plane, dx, c], sb.at[plane, dx, c], rb.at[plane, dx, c],
+            {"ep": z * nx + beside(dx)},
+        )
+
+    def project(plane, first, last, own):
+        skip = 1 if own else 0
+        for dx in range(skip, nx):
+            src = plane * nx + beside(dx)
+            landed_a(src).wait_recv()
+            copy_a2(src).start()
         for dx in list(range(1, nx)) + [0]:
-            d = dz * nx + dx
-            if d:
-                copy_a2(d).wait_recv()
-            src = down_of(d)
-            part[dz, dx, :, :chans] = dot(cols[src], wr[...]).astype(BF16)
-            part[dz, dx, :, chans:] = dot(cols[src], wg[...]).astype(BF16)
-            if dx:
-                copy_b(dz, dx).start()
-        if k:
-            pass_on(away_first[k - 1])
-    pass_on(0)
-    for dz in range(1, nz):
-        copy_bz(dz).wait_recv()
+            src = plane * nx + beside(dx)
+            if dx >= skip:
+                copy_a2(src).wait_recv()
+            for c in range(nc):
+                cs = slice(c * bw, (c + 1) * bw)
+                part[plane, dx, c, :, :bw] = dot(cols[src], wr[:, cs]).astype(BF16)
+                part[plane, dx, c, :, bw:] = dot(cols[src], wg[:, cs]).astype(BF16)
+                if dx and first <= c < last:
+                    copy_x(plane, dx, c).start()
+
+    project(z, 0, nc // 2, True)
+
+    @pl.loop(0, nz - 1)
+    def _(j):
+        project(far(j), 0, nc, False)
+
+    for c in range(nc // 2, nc):
+        for dx in range(1, nx):
+            copy_x(z, dx, c).start()
+
+    def copy_z(side, plane, c):
+        to = z + 1 - 2 * side
+        return remote(
+            zsend.at[plane, c], rz.at[side, plane, c], sz.at[plane, c], rzs.at[side, plane, c],
+            {"ep": to * nx + x},
+        )
+
+    def summed(side, plane, c):
+        for dx in range(1, nx):
+            copy_x(plane, dx, c).wait_recv()
+        total = part[plane, 0, c].astype(F32)
+        for dx in range(1, nx):
+            total = total + bx[plane, dx, c].astype(F32)
+        for s in side:
+            origin = z - 1 + 2 * s
+
+            @pl.when((origin >= 0) & (origin < nz))
+            def _():
+                copy_z(s, plane, c).wait_recv()
+
+            total = total + rz[s, plane, c].astype(F32)
+        return total
+
+    @pl.loop(0, nz - 1)
+    def _(j):
+        plane = far(j)
+        side = (plane < z).astype(jnp.int32)
+        for c in range(nc):
+            zsend[plane, c] = summed([side], plane, c).astype(BF16)
+            copy_z(side, plane, c).start()
+
+    def block(i):
+        return pl.ds(pl.multiple_of(i * share, share), share)
 
     loads[2].wait()
     loads[3].wait()
-    bw = rate_h.shape[1]
-    for b in range(rate_h.shape[0]):
-        cs = slice(b * bw, (b + 1) * bw)
-        cy = slice(chans + b * bw, chans + (b + 1) * bw)
-        proj_x = rbuf[0, :, cs].astype(F32)
-        proj_y = rbuf[0, :, cy].astype(F32)
-        for j in range(1, nz):
-            proj_x = proj_x + rbuf[j, :, cs].astype(F32)
-            proj_y = proj_y + rbuf[j, :, cy].astype(F32)
-        moved = proj_x.astype(BF16)
+    loads[4].wait()
+    for c in range(nc):
+        cs = slice(c * bw, (c + 1) * bw)
+        proj = summed([0, 1], z, c)
+        moved = proj[:, :bw].astype(BF16)
         moved_out[:, cs] = moved
         taps = conv_w[:, cs].astype(F32)
         hist = conv_in[0, :, cs].astype(F32) * taps[0:1]
         for i in range(1, 3):
             hist = hist + conv_in[i, :, cs].astype(F32) * taps[i:i + 1]
         conv = (hist + moved.astype(F32) * taps[3:4]).astype(BF16)
-        rate = jax.nn.sigmoid(dot(conv, wrate[b]))
-        in_gate = jax.nn.sigmoid(dot(conv, winput[b]))
+        rate = jax.nn.sigmoid(dot(conv, wrate[c]))
+        in_gate = jax.nn.sigmoid(dot(conv, winput[c]))
         log_decay = -8.0 * rate * jnp.log1p(jnp.exp(-rate_param[:, cs]))
         th = jnp.tanh(log_decay)
         rest = -2.0 * th / (1.0 - th)
         state = jnp.exp(log_decay) * state_in[:, cs] + jnp.sqrt(rest) * in_gate * conv.astype(F32)
         state_out[:, cs] = state
-        gated[:, cs] = (state * jax.nn.gelu(proj_y, approximate=True)).astype(BF16)
-
-    def block(i):
-        return pl.ds(pl.multiple_of(i * share, share), share)
-
-    loads[4].wait()
+        gated[:, cs] = (state * jax.nn.gelu(proj[:, bw:], approximate=True)).astype(BF16)
+        if c < nc - 1:
+            for i in range(p):
+                os = slice(i * share, (i + 1) * share)
+                piece = dot(gated[:, cs], wout[cs, os])
+                oacc[i] = piece if c == 0 else oacc[i] + piece
+
+    last = slice((nc - 1) * bw, nc * bw)
+
+    def out_part(i):
+        piece = dot(gated[:, last], wout[last, block(i)])
+        return oacc[i] + piece if nc > 1 else piece
 
     def copy_d1(yy):
         return remote(op_p.at[yy], op_r.at[yy], sd1.at[yy], rd1.at[yy], {"tp": q})
@@ -225,11 +271,11 @@
 
     for dy in range(ys):
         yy = lax.rem(y + dy + 1, ys)
-        op_p[yy] = dot(gated[...], wout[:, block(yy * 2 + 1 - core)]).astype(BF16)
+        op_p[yy] = out_part(yy * 2 + 1 - core).astype(BF16)
         copy_d1(yy).start()
     for dy in range(ys):
         yy = lax.rem(y + dy + 1, ys)
-        op_o[yy] = dot(gated[...], wout[:, block(yy * 2 + core)])
+        op_o[yy] = out_part(yy * 2 + core)
     for dy in range(1, ys):
         ty = lax.rem(y + dy, ys)
         copy_d1(ty).wait_recv()
@@ -335,15 +381,15 @@
         peer = up(d)
         return remote(outb.at[peer], ret.at[e], se3.at[d], re3.at[d], {"ep": peer})
 
-    nc = min(256, share)
+    tile = min(256, share)
     chunk = nx * cap
 
     def down(yy, parity, dst):
-        @pl.loop(0, share // nc)
+        @pl.loop(0, share // tile)
         def _(c):
-            at = pl.ds(pl.multiple_of((yy * 2 + parity) * share + c * nc, nc), nc)
-            value = dot(hid[...], wed[:, at]).reshape(nz, chunk, nc)
-            dst[yy, :, :, pl.ds(pl.multiple_of(c * nc, nc), nc)] = value.astype(dst.dtype)
+            at = pl.ds(pl.multiple_of((yy * 2 + parity) * share + c * tile, tile), tile)
+            value = dot(hid[...], wed[:, at]).reshape(nz, chunk, tile)
+            dst[yy, :, :, pl.ds(pl.multiple_of(c * tile, tile), tile)] = value.astype(dst.dtype)
 
     for dy in list(range(1, ys)) + [0]:
         ty = lax.rem(y + dy, ys)
@@ -380,8 +426,8 @@
 
     @pl.loop(1, n)
     def _(d):
-        copy_a(d).wait_send()
-        copy_a2(d).wait_send()
+        copy_a(up(d)).wait_send()
+        copy_a2(up(d)).wait_send()
         copy_c1(d).wait_send()
         copy_e3(d).wait_send()
 
@@ -399,11 +445,17 @@
         copy_d2(dy).wait_send()
         for dz in range(nz):
             copy_e2(dy, dz).wait_send()
-    for dz in range(nz):
-        for dx in range(1, nx):
-            copy_b(dz, dx).wait_send()
-        if dz:
-            copy_bz(dz).wait_send()
+    @pl.loop(0, nz)
+    def _(plane):
+        for c in range(nc):
+            for dx in range(1, nx):
+                copy_x(plane, dx, c).wait_send()
+
+    @pl.loop(0, nz - 1)
+    def _(j):
+        plane = far(j)
+        for c in range(nc):
+            copy_z((plane < z).astype(jnp.int32), plane, c).wait_send()
 
 
 def finish(layer_in, state_in, moved, conv_in, layer_out, state_out, conv_out):
@@ -430,6 +482,7 @@
     nx = 1 << ((n.bit_length() - 1) // 2)
     nx = nx if n % nx == 0 else 1
     nz = n // nx
+    nc, cw = rate_weight.shape[0], 2 * rate_weight.shape[1]
     conv_t = jnp.transpose(conv_in, (1, 0, 2))
     vm = pl.BlockSpec(memory_space=pltpu.VMEM)
     hb = pl.BlockSpec(memory_space=pl.ANY)
@@ -441,9 +494,9 @@
         V(expert_gate.shape[1:], BF16), V(expert_up.shape[1:], BF16), V(expert_down.shape[1:], BF16),
         V((1, width), F32), V((1, width), F32),
         V((n, g, depth), BF16), V((n, g, depth), BF16),
-        V((nz, nx, g, 2 * chans), BF16), V((nz, nx, g, 2 * chans), BF16),
-        V((nz, g, 2 * chans), BF16), V((nz, g, 2 * chans), BF16),
-        V((g, chans), BF16),
+        V((nz, nx, nc, g, cw), BF16), V((nz, nx, nc, g, cw), BF16),
+        V((nz, nc, g, cw), BF16), V((2, nz, nc, g, cw), BF16),
+        V((g, chans), BF16), V((p, g, share), F32),
         V((ys, g, share), BF16), V((ys, g, share), F32), V((ys, g, share), BF16),
         V((ys, g, share), BF16), V((ys, g, share), BF16), V((g, share), F32),
         V((n, cap, share), BF16), V((p, n, cap, share), BF16), V((slots, width), BF16), V((slots, hidden), BF16),
@@ -451,7 +504,7 @@
         V((ys, nz, nx * cap, share), BF16), V((ys, nz, nx * cap, share), BF16),
         V((n, cap, share), BF16), V((n, cap, share), BF16),
         dma((8,)),
-        dma((n,)), dma((n,)), dma((n,)), dma((n,)), dma((nz, nx)), dma((nz, nx)), dma((nz,)), dma((nz,)),
+        dma((n,)), dma((n,)), dma((n,)), dma((n,)), dma((nz, nx, nc)), dma((nz, nx, nc)), dma((nz, nc)), dma((2, nz, nc)),
         dma((ys,)), dma((ys,)), dma((ys,)), dma((ys,)),
         dma((n,)), dma((n,)), dma((ys, n)), dma((ys, n)), dma((ys, n)), dma((ys, n)),
         dma((ys,)), dma((ys,)), dma((ys, nz)), dma((ys, nz)), dma((n,)), dma((n,)),

time: 105 us -> 99.4 us (0.947)
  Pallas kernels: 104 us -> 98.6 us
    pallas_call x1, Pallas kernels: 102 us -> 96.5 us  [shards(): pl.pallas_call(functools.partial(kernel, n, p, nx, cap), out_shape=(jax.S...]
where the time goes in v1:
time: 99.4 us; the launch traced here: 99.2 us
  Pallas kernels  98.6 us (99%)
    pallas_call x1, Pallas kernels, shards(): pl.pallas_call(functools.partial(kernel, n, p, nx, cap), out_shape=(jax.S...  96.5 us
    pallas_call x1, Pallas kernels, shards(): pl.pallas_call(finish, out_shape=(jax.ShapeDtypeStruct(layer.shape, layer...  2.1 us

profile of v1, /device:TPU:0, one launch (start us, length us, event | category | flops | bytes accessed | tf_op | source)
XLA Modules:
  0.0 99.2 jit_solution(1635185685387296235)
XLA Ops:
  0.6 96.5 %shard_map.184 = (bf16[64,1024]{1,0:T(8,128)(2,1)}, f32[64,1024]{1,0:T(8,128)}, bf16[64,1024]{1,0:T(8,128)(2,1)}) custom-call(bf16[64,4096]{1,0:T(8,128)(2,1)} %tokens.1, f32[64,1024]{1,0:T(8,128)} %state_in.1, bf16[3,64,1024]{2,1,0:T(8,128)(2,1)} %bitcast.7, bf16[32,128]{1,0:T(8,128)(2,1)} %bitcast.9, bf16[32,128]{1,0:T(8,128)(2,1)} %bitcast.10, ...), custom_call_target="tpu_custom_call" | custom-call | tf_op jit(solution)/shard_map/pallas_call | solution.py:512
  97.1 2.1 %shard_map.185 = (bf16[64,1024]{1,0:T(8,128)(2,1)}, f32[64,1024]{1,0:T(8,128)}, bf16[3,64,1024]{2,1,0:T(8,128)(2,1)}) custom-call(bf16[64,1024]{1,0:T(8,128)(2,1)} %get-tuple-element.9.layer_in, f32[64,1024]{1,0:T(8,128)} %get-tuple-element.10.state_in, bf16[64,1024]{1,0:T(8,128)(2,1)} %get-tuple-element.11.moved, bf16[3,64,1024]{2,1,0:T(8,128)(2,1)} %bitcast.8), custom_call_target="tpu_custom_call" | custom-call | tf_op jit(solution)/shard_map/pallas_call | solution.py:530

commit v2 on v1

v2 whole, which is shorter than its diff:
```python
import functools

import jax
import jax.numpy as jnp
from jax import lax
from jax.experimental import pallas as pl
from jax.experimental.pallas import tpu as pltpu
from jax.sharding import PartitionSpec as P

MESH = pl.DeviceIdType.MESH
F32 = jnp.float32
BF16 = jnp.bfloat16
HALVES = 2
LAG = 3


def dot(a, b):
    return jnp.dot(a, b, preferred_element_type=F32)


def remote(src, dst, send, recv, where):
    return pltpu.make_async_remote_copy(
        src_ref=src, dst_ref=dst, send_sem=send, recv_sem=recv, device_id=where, device_id_type=MESH
    )


def kernel(
    n, p, nx, cap,
    tokens_h, state_h, conv_h, mix_h, moe_h, taps_h, param_h, routes_h, prob_h,
    rnn_h, gate_h, rate_h, input_h, out_h, eg_h, eu_h, ed_h,
    layer_out, state_out, conv_out,
    tokens, state_in, conv_in, mix_gain_in, moe_gain_in, conv_w, rate_param, routes, prob,
    layer_v, state_v, conv_v,
    wr, wg, wrate, winput, wout, weg, weu, wed,
    mix_gain, moe_gain, normed, cols, part, bx, zsend, rz, gated, oacc,
    op_p, op_o, op_r, hs, hr, mixed,
    sd, rows, xn, ssq, gacc, hid, e_p, e_o, e_r, es, er, outb, ret,
    wsem, lsem, osem, sa, ra, sa2, ra2, sb, rb, sz, rzs, sd1, rd1, sd2, rd2,
    sc1, rc1, sc2, rc2, sc3, rc3, se1, re1, se2, re2, se3, re3,
):
    e = lax.axis_index("ep")
    t = lax.axis_index("tp")
    core = lax.rem(t, 2)
    y = t // 2
    q = t + 1 - 2 * core
    ys = p // 2
    nz = n // nx
    z = e // nx
    x = lax.rem(e, nx)

    rows_g, width = tokens.shape
    depth = width // n
    share = width // p
    sw = share // HALVES
    slots = n * cap

    small = [
        pltpu.make_async_copy(a, b, lsem.at[i])
        for i, (a, b) in enumerate(
            [(tokens_h, tokens), (mix_h, mix_gain_in), (moe_h, moe_gain_in), (routes_h, routes), (prob_h, prob),
             (taps_h, conv_w), (param_h, rate_param), (conv_h, conv_in), (state_h, state_in)]
        )
    ]
    loads = [
        pltpu.make_async_copy(a, b, wsem.at[i])
        for i, (a, b) in enumerate(
            [(rnn_h, wr), (gate_h, wg), (rate_h, wrate), (input_h, winput), (out_h, wout),
             (eg_h.at[0], weg), (eu_h.at[0], weu), (ed_h.at[0], wed)]
        )
    ]
    small[0].start()
    small[1].start()

    barrier = pltpu.get_barrier_semaphore()

    @pl.loop(1, n)
    def _(d):
        pl.semaphore_signal(barrier, inc=1, device_id={"ep": lax.rem(e + d, n)}, device_id_type=MESH)

    @pl.loop(1, p)
    def _(d):
        pl.semaphore_signal(barrier, inc=1, device_id={"tp": lax.rem(t + d, p)}, device_id_type=MESH)

    for load in small[2:] + loads[:4]:
        load.start()

    @pl.when(z == 0)
    def _():
        rz[0] = jnp.zeros(rz.shape[1:], BF16)

    @pl.when(z == nz - 1)
    def _():
        rz[1] = jnp.zeros(rz.shape[1:], BF16)

    small[0].wait()
    small[1].wait()
    for j in range(width // 128):
        cs = slice(j * 128, (j + 1) * 128)
        mix_gain[:, cs] = mix_gain_in[j:j + 1, :].astype(F32)

    total_sq = jnp.zeros((rows_g, 1), F32)
    for j in range(n):
        v = tokens[:, j * depth:(j + 1) * depth].astype(F32)
        total_sq = total_sq + jnp.sum(v * v, axis=1, keepdims=True)
    scale = lax.rsqrt(total_sq / width + 1e-06)
    for j in range(n):
        cs = slice(j * depth, (j + 1) * depth)
        normed[j] = (tokens[:, cs].astype(F32) * scale * mix_gain[:, cs]).astype(BF16)

    pl.semaphore_wait(barrier, n + p - 2)

    half = pl.ds(pl.multiple_of(core * (rows_g // 2), rows_g // 2), rows_g // 2)
    nc, bw = rate_h.shape[0], rate_h.shape[1]
    high = (2 * z) // nz
    folded = z + high * (nz - 1 - 2 * z)

    def far(j):
        plane = nz - 1 - j
        plane = plane - (folded >= plane).astype(jnp.int32)
        return plane + high * (nz - 1 - 2 * plane)

    def beside(dx):
        return lax.rem(x + dx, nx)

    def peer_of(plane, dx):
        return plane * nx + beside(dx)

    def copy_a(peer):
        return remote(normed.at[peer, half], cols.at[e, half], sa.at[peer], ra.at[e], {"ep": peer})

    def landed_a(src):
        return remote(normed.at[src, half], cols.at[src, half], sa.at[src], ra.at[src], {"ep": src})

    def copy_a2(src):
        return remote(cols.at[src, half], cols.at[src, half], sa2.at[src], ra2.at[src], {"tp": q})

    for dx in range(1, nx):
        copy_a(peer_of(z, dx)).start()

    @pl.loop(0, nz - 1)
    def _(j):
        for dx in range(nx):
            copy_a(peer_of(far(j), dx)).start()

    cols[e] = normed[e]

    for j in range(2, 5):
        small[j].wait()
    for j in range(width // 128):
        cs = slice(j * 128, (j + 1) * 128)
        moe_gain[:, cs] = moe_gain_in[j:j + 1, :].astype(F32)
    ids = routes[...]
    sub_e = lax.broadcasted_iota(jnp.int32, (n, rows_g), 0)
    named = [(ids[k:k + 1, :] == sub_e).astype(F32) for k in range(ids.shape[0])]
    member = functools.reduce(lambda a, b: a + b, named)
    earlier = (
        lax.broadcasted_iota(jnp.int32, (rows_g, rows_g), 0)
        < lax.broadcasted_iota(jnp.int32, (rows_g, rows_g), 1)
    ).astype(F32)
    before = dot(member.astype(BF16), earlier.astype(BF16))
    sub_s = lax.broadcasted_iota(jnp.int32, (slots, rows_g), 0).astype(F32)
    total_prob = jnp.sum(prob[...], axis=0, keepdims=True)
    dispatch = jnp.zeros((slots, rows_g), F32)
    comb = jnp.zeros((slots, rows_g), F32)
    for k in range(ids.shape[0]):
        slot = jnp.sum(before * named[k], axis=0, keepdims=True)
        target = ids[k:k + 1, :].astype(F32) * cap + slot
        hit = (sub_s == target).astype(F32)
        dispatch = dispatch + hit
        comb = comb + hit * (prob[k:k + 1, :] / total_prob)
    dispatch = dispatch.astype(BF16)
    comb_hi = comb.astype(BF16)
    comb_lo = (comb - comb_hi.astype(F32)).astype(BF16)

    loads[0].wait()
    loads[1].wait()
    for load in loads[4:]:
        load.start()

    def copy_x(plane, dx, c):
        return remote(
            part.at[plane, beside(dx), c], bx.at[plane, dx, c], sb.at[plane, dx, c], rb.at[plane, dx, c],
            {"ep": peer_of(z, dx)},
        )

    def project(plane, last, own):
        first = 1 if own else 0
        for dx in range(first, nx):
            src = peer_of(plane, dx)
            landed_a(src).wait_recv()
            copy_a2(src).start()
        for dx in range(first, nx):
            copy_a2(peer_of(plane, dx)).wait_recv()
        feats = cols[pl.ds(plane * nx, nx)].reshape(nx * rows_g, depth)
        for c in range(nc):
            cs = slice(c * bw, (c + 1) * bw)
            for lo, weight in ((0, wr), (bw, wg)):
                value = dot(feats, weight[:, cs]).astype(BF16)
                for i in range(nx):
                    part[plane, i, c, :, lo:lo + bw] = value[i * rows_g:(i + 1) * rows_g]
            if c < last:
                for dx in range(1, nx):
                    copy_x(plane, dx, c).start()

    project(z, nc // 2, True)

    @pl.loop(0, nz - 1)
    def _(j):
        project(far(j), nc, False)

    for c in range(nc // 2, nc):
        for dx in range(1, nx):
            copy_x(z, dx, c).start()

    def copy_z(side, plane, c):
        to = z + 1 - 2 * side
        return remote(
            zsend.at[plane, c], rz.at[side, plane, c], sz.at[plane, c], rzs.at[side, plane, c],
            {"ep": to * nx + x},
        )

    def summed(sides, plane, c):
        for dx in range(1, nx):
            copy_x(plane, dx, c).wait_recv()
        total = part[plane, x, c].astype(F32)
        for dx in range(1, nx):
            total = total + bx[plane, dx, c].astype(F32)
        for s in sides:
            origin = z - 1 + 2 * s

            @pl.when((origin >= 0) & (origin < nz))
            def _():
                copy_z(s, plane, c).wait_recv()

            total = total + rz[s, plane, c].astype(F32)
        return total

    @pl.loop(0, nz - 1)
    def _(j):
        plane = far(j)
        side = (plane < z).astype(jnp.int32)
        for c in range(nc):
            zsend[plane, c] = summed([side], plane, c).astype(BF16)
            copy_z(side, plane, c).start()

    def block(i, h):
        return pl.ds(pl.multiple_of(i * share + h * sw, sw), sw)

    for load in small[5:]:
        load.wait()
    loads[2].wait()
    loads[3].wait()
    loads[4].wait()
    for i in range(1, conv_in.shape[0]):
        conv_v[i - 1] = conv_in[i]
    for c in range(nc):
        cs = slice(c * bw, (c + 1) * bw)
        proj = summed([0, 1], z, c)
        moved = proj[:, :bw].astype(BF16)
        conv_v[conv_in.shape[0] - 1, :, cs] = moved
        taps = conv_w[:, cs].astype(F32)
        hist = conv_in[0, :, cs].astype(F32) * taps[0:1]
        for i in range(1, 3):
            hist = hist + conv_in[i, :, cs].astype(F32) * taps[i:i + 1]
        conv = (hist + moved.astype(F32) * taps[3:4]).astype(BF16)
        rate = jax.nn.sigmoid(dot(conv, wrate[c]))
        in_gate = jax.nn.sigmoid(dot(conv, winput[c]))
        log_decay = -8.0 * rate * jnp.log1p(jnp.exp(-rate_param[:, cs]))
        th = jnp.tanh(log_decay)
        rest = -2.0 * th / (1.0 - th)
        state = jnp.exp(log_decay) * state_in[:, cs] + jnp.sqrt(rest) * in_gate * conv.astype(F32)
        state_v[:, cs] = state
        gated[:, cs] = (state * jax.nn.gelu(proj[:, bw:], approximate=True)).astype(BF16)
        if c < nc - 1:
            for i in range(p):
                for h in range(HALVES):
                    lo = i * share + h * sw
                    piece = dot(gated[:, cs], wout[cs, lo:lo + sw])
                    oacc[i, h] = piece if c == 0 else oacc[i, h] + piece

    last = slice((nc - 1) * bw, nc * bw)

    def out_part(i, h):
        piece = dot(gated[:, last], wout[last, block(i, h)])
        return oacc[i, h] + piece if nc > 1 else piece

    def copy_d1(yy, h):
        return remote(op_p.at[yy, h], op_r.at[yy, h], sd1.at[yy, h], rd1.at[yy, h], {"tp": q})

    def copy_d2(dy, h):
        ty = lax.rem(y + dy, ys)
        return remote(hs.at[ty, h], hr.at[y, h], sd2.at[dy, h], rd2.at[dy, h], {"tp": ty * 2 + core})

    for dy in range(ys):
        yy = lax.rem(y + dy + 1, ys)
        for h in range(HALVES):
            op_p[yy, h] = out_part(yy * 2 + 1 - core, h).astype(BF16)
            copy_d1(yy, h).start()
    for dy in range(ys):
        yy = lax.rem(y + dy + 1, ys)
        for h in range(HALVES):
            op_o[yy, h] = out_part(yy * 2 + core, h)
    for h in range(HALVES):
        for dy in range(1, ys):
            ty = lax.rem(y + dy, ys)
            copy_d1(ty, h).wait_recv()
            hs[ty, h] = (op_o[ty, h] + op_r[ty, h].astype(F32)).astype(BF16)
            copy_d2(dy, h).start()

    puts = [
        pltpu.make_async_copy(a, b, osem.at[i])
        for i, (a, b) in enumerate([(state_v, state_out), (conv_v, conv_out), (layer_v, layer_out)])
    ]
    puts[0].start()
    puts[1].start()

    def copy_c1(peer, h):
        return remote(sd.at[peer, h], rows.at[t, e, h], sc1.at[peer, h], rc1.at[e, h], {"ep": peer})

    def landed_c1(src, h):
        return remote(sd.at[src, h], rows.at[t, src, h], sc1.at[src, h], rc1.at[src, h], {"ep": src})

    def copy_c2(dy, src, h):
        to = lax.rem(y + dy, ys) * 2 + core
        return remote(rows.at[t, src, h], rows.at[t, src, h], sc2.at[dy, src, h], rc2.at[dy, src, h], {"tp": to})

    def landed_c2(dy, src, h):
        held = lax.rem(y - dy + ys, ys) * 2 + core
        return remote(
            rows.at[held, src, h], rows.at[held, src, h], sc2.at[dy, src, h], rc2.at[dy, src, h], {"tp": held}
        )

    def copy_c3(dy, src, h):
        held = lax.rem(y - dy + ys, ys) * 2 + core
        return remote(
            rows.at[held, src, h], rows.at[held, src, h], sc3.at[dy, src, h], rc3.at[dy, src, h], {"tp": q}
        )

    def landed_c3(dy, src, h):
        held = lax.rem(y - dy + ys, ys) * 2 + 1 - core
        return remote(
            rows.at[held, src, h], rows.at[held, src, h], sc3.at[dy, src, h], rc3.at[dy, src, h], {"tp": q}
        )

    for h in range(HALVES):
        copy_d1(y, h).wait_recv()
        total = tokens[:, block(t, h)].astype(F32) + op_o[y, h] + op_r[y, h].astype(F32)
        for dy in range(1, ys):
            copy_d2(dy, h).wait_recv()
            total = total + hr[lax.rem(y - dy + ys, ys), h].astype(F32)
        mixed[h] = total
        sent = dot(dispatch, total.astype(BF16)).reshape(n, cap, sw).astype(BF16)
        for i in range(n):
            sd[i, h] = sent[i]
        for dx in range(1, nx):
            copy_c1(peer_of(z, dx), h).start()

        @pl.loop(0, nz - 1)
        def _(j):
            for dx in range(nx):
                copy_c1(peer_of(far(j), dx), h).start()

        rows[t, e, h] = sd[e, h]
        for dy in range(1, ys):
            copy_c2(dy, e, h).start()
        copy_c3(0, e, h).start()

    gs = min(n, max(1, 64 // cap))
    span = gs * cap
    hidden = hid.shape[1]
    fc = min(256, hidden)

    def scaled_rows(h):
        @pl.loop(0, n)
        def _(src):
            for dy in range(ys):
                landed_c3(dy, src, h).wait_recv()

        @pl.loop(0, n // gs)
        def _(g):
            at = pl.ds(pl.multiple_of(g * span, span), span)
            acc = jnp.zeros((span, 1), F32)
            for i in range(p):
                lo = i * share + h * sw
                v = rows[i, pl.ds(g * gs, gs), h].astype(F32).reshape(span, sw)
                acc = acc + jnp.sum(v * v, axis=1, keepdims=True)
                xn[h, at, i * sw:(i + 1) * sw] = (v * moe_gain[:, lo:lo + sw]).astype(BF16)
            ssq[at, :] = acc if h == 0 else ssq[at, :] + acc

    def partial_dot(weight, h, cs):
        acc = None
        for i in range(p):
            lo = i * share + h * sw
            piece = dot(xn[h, :, i * sw:(i + 1) * sw], weight[lo:lo + sw, cs])
            acc = piece if acc is None else acc + piece
        return acc

    def early(k, weight, f):
        cs = slice(f * fc, (f + 1) * fc)
        gacc[k, :, cs] = partial_dot(weight, 0, cs)

    def first_half():
        loads[5].wait()
        loads[6].wait()
        scaled_rows(0)

    tasks = [first_half]
    for f in range(hidden // fc):
        tasks.append(functools.partial(early, 0, weg, f))
        tasks.append(functools.partial(early, 1, weu, f))

    near = [(z, dx) for dx in range(1, nx)]
    near = near + [(far(j), dx) for j in reversed(range(nz - 1)) for dx in range(nx)]
    steps = [(peer_of(plane, dx), h) for h in range(HALVES) for plane, dx in near]
    queue = [(e, h) for h in range(HALVES)]
    begin = len(near) + len(near) // 2
    for i, (src, h) in enumerate(steps):
        landed_c1(src, h).wait_recv()
        for dy in range(1, ys):
            copy_c2(dy, src, h).start()
        copy_c3(0, src, h).start()
        queue.append((src, h))
        if len(queue) > LAG:
            was, wh = queue.pop(0)
            for dy in range(1, ys):
                landed_c2(dy, was, wh).wait_recv()
                copy_c3(dy, was, wh).start()
        if i >= begin and tasks:
            tasks.pop(0)()
    for was, wh in queue:
        for dy in range(1, ys):
            landed_c2(dy, was, wh).wait_recv()
            copy_c3(dy, was, wh).start()
    for task in tasks:
        task()

    scaled_rows(HALVES - 1)
    row_scale = lax.rsqrt(ssq[...] / width + 1e-06)
    for f in range(hidden // fc):
        cs = slice(f * fc, (f + 1) * fc)
        gate_part = (gacc[0, :, cs] + partial_dot(weg, 1, cs)) * row_scale
        up_part = (gacc[1, :, cs] + partial_dot(weu, 1, cs)) * row_scale
        hid[:, cs] = (jax.nn.silu(gate_part) * up_part).astype(BF16)

    loads[7].wait()
    chunk = nx * cap

    def copy_e1(plane, yy):
        return remote(e_p.at[plane, yy], e_r.at[plane, yy], se1.at[plane, yy], re1.at[plane, yy], {"tp": q})

    def copy_e2(plane, dy, h):
        ty = lax.rem(y + dy, ys)
        return remote(
            es.at[plane, ty, h], er.at[plane, y, h], se2.at[plane, dy, h], re2.at[plane, dy, h],
            {"tp": ty * 2 + core},
        )

    def copy_e3(peer, h):
        return remote(outb.at[peer, h], ret.at[e, h], se3.at[peer, h], re3.at[e, h], {"ep": peer})

    def landed_e3(src, h):
        return remote(outb.at[src, h], ret.at[src, h], se3.at[src, h], re3.at[src, h], {"ep": src})

    def issue(plane):
        mine = hid[pl.ds(pl.multiple_of(plane * chunk, chunk), chunk), :]
        for dy in list(range(1, ys)) + [0]:
            ty = lax.rem(y + dy, ys)
            for h in range(HALVES):
                e_p[plane, ty, h] = dot(mine, wed[:, block(ty * 2 + 1 - core, h)]).astype(BF16)
            copy_e1(plane, ty).start()
            for h in range(HALVES):
                e_o[plane, ty, h] = dot(mine, wed[:, block(ty * 2 + core, h)])

    def push(plane):
        for dy in range(1, ys):
            ty = lax.rem(y + dy, ys)
            copy_e1(plane, ty).wait_recv()
            for h in range(HALVES):
                es[plane, ty, h] = (e_o[plane, ty, h] + e_r[plane, ty, h].astype(F32)).astype(BF16)
                copy_e2(plane, dy, h).start()

    def deliver(plane, first):
        copy_e1(plane, y).wait_recv()
        for h in range(HALVES):
            result = e_o[plane, y, h] + e_r[plane, y, h].astype(F32)
            for dy in range(1, ys):
                copy_e2(plane, dy, h).wait_recv()
                result = result + er[plane, lax.rem(y - dy + ys, ys), h].astype(F32)
            result = result.reshape(nx, cap, sw).astype(BF16)
            for i in range(nx):
                outb[plane * nx + i, h] = result[i]
            for dx in range(first, nx):
                copy_e3(peer_of(plane, dx), h).start()

    @pl.loop(0, nz - 1)
    def _(j):
        issue(far(j))

        @pl.when(j > 0)
        def _():
            push(far(j - 1))

    issue(z)
    if nz > 1:
        push(far(nz - 2))
    push(z)

    @pl.loop(0, nz - 1)
    def _(j):
        deliver(far(j), 0)

    deliver(z, 1)
    for h in range(HALVES):
        ret[e, h] = outb[e, h]

    def combine(weights, back):
        return lax.dot_general(weights, back, (((0,), (0,)), ((), ())), preferred_element_type=F32)

    for h in range(HALVES):
        @pl.loop(1, n)
        def _(d):
            landed_e3(lax.rem(e + d, n), h).wait_recv()

        back = jnp.concatenate([ret[i, h] for i in range(n)], axis=0)
        layer_v[:, h * sw:(h + 1) * sw] = (
            mixed[h] + combine(comb_hi, back) + combine(comb_lo, back)
        ).astype(BF16)

    puts[2].start()

    @pl.loop(1, n)
    def _(d):
        peer = lax.rem(e + d, n)
        copy_a(peer).wait_send()
        copy_a2(peer).wait_send()
        for h in range(HALVES):
            copy_c1(peer, h).wait_send()
            copy_e3(peer, h).wait_send()

    @pl.loop(0, n)
    def _(src):
        for h in range(HALVES):
            for dy in range(1, ys):
                copy_c2(dy, src, h).wait_send()
            for dy in range(ys):
                copy_c3(dy, src, h).wait_send()

    for dy in range(ys):
        for h in range(HALVES):
            copy_d1(dy, h).wait_send()
            if dy:
                copy_d2(dy, h).wait_send()

    @pl.loop(0, nz)
    def _(plane):
        for yy in range(ys):
            copy_e1(plane, yy).wait_send()
        for dy in range(1, ys):
            for h in range(HALVES):
                copy_e2(plane, dy, h).wait_send()
        for c in range(nc):
            for dx in range(1, nx):
                copy_x(plane, dx, c).wait_send()

    @pl.loop(0, nz - 1)
    def _(j):
        plane = far(j)
        for c in range(nc):
            copy_z((plane < z).astype(jnp.int32), plane, c).wait_send()

    for put in puts:
        put.wait()


def finish(layer_in, state_in, conv_in, layer_out, state_out, conv_out):
    layer_out[...] = layer_in[...]
    state_out[...] = state_in[...]
    conv_out[...] = conv_in[...]


def shards(
    n, p,
    tokens, state_in, conv_in, mix_gain, rnn_weight, gate_weight, conv_weight, rate_weight,
    input_weight, rate_param, out_weight, moe_gain, expert_gate, expert_up, expert_down, routes, route_prob,
):
    g, width = tokens.shape
    depth, chans = rnn_weight.shape
    share = width // p
    cap = max(2, 2 * g * routes.shape[1] // n)
    slots = n * cap
    hidden = expert_gate.shape[2]
    ys = p // 2
    nx = 1 << ((n.bit_length() - 1) // 2)
    nx = nx if n % nx == 0 else 1
    nz = n // nx
    nc, cw = rate_weight.shape[0], 2 * rate_weight.shape[1]
    nh, sw = HALVES, share // HALVES
    chunk = nx * cap
    vm = pl.BlockSpec(memory_space=pltpu.VMEM)
    hb = pl.BlockSpec(memory_space=pl.ANY)
    dma = pltpu.SemaphoreType.DMA
    V = pltpu.VMEM
    small = (
        tokens, state_in, jnp.transpose(conv_in, (1, 0, 2)), mix_gain.reshape(-1, 128), moe_gain.reshape(-1, 128),
        conv_weight, rate_param[None], routes.T, route_prob.T,
    )
    scratch = [V(a.shape, a.dtype) for a in small] + [
        V((g, share), BF16), V((g, chans), F32), V((conv_in.shape[1], g, chans), BF16),
        V((depth, chans), BF16), V((depth, chans), BF16),
        V(rate_weight.shape, BF16), V(input_weight.shape, BF16), V(out_weight.shape, BF16),
        V(expert_gate.shape[1:], BF16), V(expert_up.shape[1:], BF16), V(expert_down.shape[1:], BF16),
        V((1, width), F32), V((1, width), F32),
        V((n, g, depth), BF16), V((n, g, depth), BF16),
        V((nz, nx, nc, g, cw), BF16), V((nz, nx, nc, g, cw), BF16),
        V((nz, nc, g, cw), BF16), V((2, nz, nc, g, cw), BF16),
        V((g, chans), BF16), V((p, nh, g, sw), F32),
        V((ys, nh, g, sw), BF16), V((ys, nh, g, sw), F32), V((ys, nh, g, sw), BF16),
        V((ys, nh, g, sw), BF16), V((ys, nh, g, sw), BF16), V((nh, g, sw), F32),
        V((n, nh, cap, sw), BF16), V((p, n, nh, cap, sw), BF16), V((nh, slots, p * sw), BF16), V((slots, 1), F32),
        V((2, slots, hidden), F32), V((slots, hidden), BF16),
        V((nz, ys, nh, chunk, sw), BF16), V((nz, ys, nh, chunk, sw), F32), V((nz, ys, nh, chunk, sw), BF16),
        V((nz, ys, nh, chunk, sw), BF16), V((nz, ys, nh, chunk, sw), BF16),
        V((n, nh, cap, sw), BF16), V((n, nh, cap, sw), BF16),
        dma((8,)), dma((len(small),)), dma((3,)),
        dma((n,)), dma((n,)), dma((n,)), dma((n,)),
        dma((nz, nx, nc)), dma((nz, nx, nc)), dma((nz, nc)), dma((2, nz, nc)),
        dma((ys, nh)), dma((ys, nh)), dma((ys, nh)), dma((ys, nh)),
        dma((n, nh)), dma((n, nh)), dma((ys, n, nh)), dma((ys, n, nh)), dma((ys, n, nh)), dma((ys, n, nh)),
        dma((nz, ys)), dma((nz, ys)), dma((nz, ys, nh)), dma((nz, ys, nh)), dma((n, nh)), dma((n, nh)),
    ]
    outs = (
        jax.ShapeDtypeStruct((g, share), BF16),
        jax.ShapeDtypeStruct((g, chans), F32),
        jax.ShapeDtypeStruct((conv_in.shape[1], g, chans), BF16),
    )
    held = pl.pallas_call(
        functools.partial(kernel, n, p, nx, cap),
        out_shape=outs,
        in_specs=[hb] * 17,
        out_specs=(hb, hb, hb),
        scratch_shapes=scratch,
        compiler_params=pltpu.CompilerParams(
            collective_id=0, has_side_effects=True, vmem_limit_bytes=60 * 1024 * 1024
        ),
    )(
        *small,
        rnn_weight, gate_weight, rate_weight, input_weight, out_weight, expert_gate, expert_up, expert_down,
    )
    layer_out, state_out, conv_out = pl.pallas_call(
        finish,
        out_shape=outs,
        in_specs=[vm] * 3,
        out_specs=(vm, vm, vm),
    )(*held)
    return (layer_out, state_out, jnp.transpose(conv_out, (1, 0, 2)))


def solution(mesh):
    in_specs = (
        P("ep", None),
        P("ep", "tp"),
        P("ep", None, "tp"),
        P(),
        P("ep", "tp"),
        P("ep", "tp"),
        P(None, "tp"),
        P("tp", None, None),
        P("tp", None, None),
        P("tp"),
        P("tp", None),
        P(),
        P("ep", None, "tp"),
        P("ep", None, "tp"),
        P("ep", "tp", None),
        P("ep", None),
        P("ep", None),
    )
    out_specs = (P("ep", "tp"), P("ep", "tp"), P("ep", None, "tp"))
    body = functools.partial(shards, mesh.shape["ep"], mesh.shape["tp"])
    return jax.shard_map(body, mesh=mesh, in_specs=in_specs, out_specs=out_specs, check_vma=False)
```

time: 99.4 us -> 91 us (0.915)
  Pallas kernels: 98.6 us -> 90.2 us
    pallas_call x2, Pallas kernels: 98.6 us -> 90.2 us  [the longest x1 88.2 us: shards(): pl.pallas_call(functools.partial(kernel, n, p, nx, cap), out_shape=outs,...]
where the time goes in v2:
time: 91 us; the launch traced here: 90.9 us
  Pallas kernels  90.2 us (99%)
    pallas_call x1, Pallas kernels, shards(): pl.pallas_call(functools.partial(kernel, n, p, nx, cap), out_shape=outs,...  88.2 us
    pallas_call x1, Pallas kernels, shards(): pl.pallas_call(finish, out_shape=outs, in_specs=[vm] * 3, out_specs=(vm,...  2.03 us

profile of v2, /device:TPU:0, one launch (start us, length us, event | category | flops | bytes accessed | tf_op | source)
XLA Modules:
  0.0 90.9 jit_solution(7473732636152463549)
XLA Ops:
  0.6 88.2 %shard_map.184 = (bf16[64,1024]{1,0:T(8,128)(2,1)}, f32[64,1024]{1,0:T(8,128)}, bf16[3,64,1024]{2,1,0:T(8,128)(2,1)}) custom-call(bf16[64,4096]{1,0:T(8,128)(2,1)} %tokens_h.1, f32[64,1024]{1,0:T(8,128)} %state_h.1, bf16[3,64,1024]{2,1,0:T(8,128)(2,1)} %bitcast.7, bf16[32,128]{1,0:T(8,128)(2,1)} %bitcast.8, bf16[32,128]{1,0:T(8,128)(2,1)} %bitcast.9, ...), custom_call_target="tpu_custom_call" | custom-call | tf_op jit(solution)/shard_map/pallas_call | solution.py:636
  88.8 2.0 %shard_map.185 = (bf16[64,1024]{1,0:T(8,128)(2,1)}, f32[64,1024]{1,0:T(8,128)}, bf16[3,64,1024]{2,1,0:T(8,128)(2,1)}) custom-call(bf16[64,1024]{1,0:T(8,128)(2,1)} %get-tuple-element.9.layer_in, f32[64,1024]{1,0:T(8,128)} %get-tuple-element.10.state_in, bf16[3,64,1024]{2,1,0:T(8,128)(2,1)} %get-tuple-element.11.conv_in), custom_call_target="tpu_custom_call" | custom-call | tf_op jit(solution)/shard_map/pallas_call | solution.py:649

commit v3 on v2

--- a/solution.py
+++ b/solution.py
@@ -126,13 +126,13 @@
         return plane * nx + beside(dx)
 
     def copy_a(peer):
-        return remote(normed.at[peer, half], cols.at[e, half], sa.at[peer], ra.at[e], {"ep": peer})
+        return remote(normed.at[peer, half], cols.at[e, half], sa, ra.at[e], {"ep": peer})
 
     def landed_a(src):
-        return remote(normed.at[src, half], cols.at[src, half], sa.at[src], ra.at[src], {"ep": src})
+        return remote(normed.at[src, half], cols.at[src, half], sa, ra.at[src], {"ep": src})
 
     def copy_a2(src):
-        return remote(cols.at[src, half], cols.at[src, half], sa2.at[src], ra2.at[src], {"tp": q})
+        return remote(cols.at[src, half], cols.at[src, half], sa2, ra2.at[src], {"tp": q})
 
     for dx in range(1, nx):
         copy_a(peer_of(z, dx)).start()
@@ -179,7 +179,7 @@
 
     def copy_x(plane, dx, c):
         return remote(
-            part.at[plane, beside(dx), c], bx.at[plane, dx, c], sb.at[plane, dx, c], rb.at[plane, dx, c],
+            part.at[plane, beside(dx), c], bx.at[plane, dx, c], sb, rb.at[plane, dx - 1, c],
             {"ep": peer_of(z, dx)},
         )
 
@@ -215,7 +215,7 @@
     def copy_z(side, plane, c):
         to = z + 1 - 2 * side
         return remote(
-            zsend.at[plane, c], rz.at[side, plane, c], sz.at[plane, c], rzs.at[side, plane, c],
+            zsend.at[plane, c], rz.at[side, plane, c], sz, rzs.at[side, plane, c],
             {"ep": to * nx + x},
         )
 
@@ -285,11 +285,11 @@
         return oacc[i, h] + piece if nc > 1 else piece
 
     def copy_d1(yy, h):
-        return remote(op_p.at[yy, h], op_r.at[yy, h], sd1.at[yy, h], rd1.at[yy, h], {"tp": q})
+        return remote(op_p.at[yy, h], op_r.at[yy, h], sd1, rd1.at[yy, h], {"tp": q})
 
     def copy_d2(dy, h):
         ty = lax.rem(y + dy, ys)
-        return remote(hs.at[ty, h], hr.at[y, h], sd2.at[dy, h], rd2.at[dy, h], {"tp": ty * 2 + core})
+        return remote(hs.at[ty, h], hr.at[y, h], sd2, rd2.at[dy - 1, h], {"tp": ty * 2 + core})
 
     for dy in range(ys):
         yy = lax.rem(y + dy + 1, ys)
@@ -315,31 +315,25 @@
     puts[1].start()
 
     def copy_c1(peer, h):
-        return remote(sd.at[peer, h], rows.at[t, e, h], sc1.at[peer, h], rc1.at[e, h], {"ep": peer})
+        return remote(sd.at[h, peer], rows.at[h, t, e], sc1, rc1.at[e, h], {"ep": peer})
 
     def landed_c1(src, h):
-        return remote(sd.at[src, h], rows.at[t, src, h], sc1.at[src, h], rc1.at[src, h], {"ep": src})
+        return remote(sd.at[h, src], rows.at[h, t, src], sc1, rc1.at[src, h], {"ep": src})
 
     def copy_c2(dy, src, h):
         to = lax.rem(y + dy, ys) * 2 + core
-        return remote(rows.at[t, src, h], rows.at[t, src, h], sc2.at[dy, src, h], rc2.at[dy, src, h], {"tp": to})
+        return remote(rows.at[h, t, src], rows.at[h, t, src], sc2, rc2.at[dy - 1, src, h], {"tp": to})
 
     def landed_c2(dy, src, h):
         held = lax.rem(y - dy + ys, ys) * 2 + core
         return remote(
-            rows.at[held, src, h], rows.at[held, src, h], sc2.at[dy, src, h], rc2.at[dy, src, h], {"tp": held}
+            rows.at[h, held, src], rows.at[h, held, src], sc2, rc2.at[dy - 1, src, h], {"tp": held}
         )
 
     def copy_c3(dy, src, h):
         held = lax.rem(y - dy + ys, ys) * 2 + core
         return remote(
-            rows.at[held, src, h], rows.at[held, src, h], sc3.at[dy, src, h], rc3.at[dy, src, h], {"tp": q}
-        )
-
-    def landed_c3(dy, src, h):
-        held = lax.rem(y - dy + ys, ys) * 2 + 1 - core
-        return remote(
-            rows.at[held, src, h], rows.at[held, src, h], sc3.at[dy, src, h], rc3.at[dy, src, h], {"tp": q}
+            rows.at[h, held, src], rows.at[h, held, src], sc3, rc3.at[h], {"tp": q}
         )
 
     for h in range(HALVES):
@@ -350,17 +344,16 @@
             total = total + hr[lax.rem(y - dy + ys, ys), h].astype(F32)
         mixed[h] = total
         sent = dot(dispatch, total.astype(BF16)).reshape(n, cap, sw).astype(BF16)
-        for i in range(n):
-            sd[i, h] = sent[i]
+        sd[h] = sent
         for dx in range(1, nx):
             copy_c1(peer_of(z, dx), h).start()
 
         @pl.loop(0, nz - 1)
         def _(j):
             for dx in range(nx):
-                copy_c1(peer_of(far(j), dx), h).start()
-
-        rows[t, e, h] = sd[e, h]
+                copy_c1(peer_of(far(nz - 2 - j), dx), h).start()
+
+        rows[h, t, e] = sd[h, e]
         for dy in range(1, ys):
             copy_c2(dy, e, h).start()
         copy_c3(0, e, h).start()
@@ -371,10 +364,8 @@
     fc = min(256, hidden)
 
     def scaled_rows(h):
-        @pl.loop(0, n)
-        def _(src):
-            for dy in range(ys):
-                landed_c3(dy, src, h).wait_recv()
+        mate = rows.at[h, pl.ds(0, ys)]
+        remote(mate, mate, sc3, rc3.at[h], {"tp": q}).wait_recv()
 
         @pl.loop(0, n // gs)
         def _(g):
@@ -382,7 +373,7 @@
             acc = jnp.zeros((span, 1), F32)
             for i in range(p):
                 lo = i * share + h * sw
-                v = rows[i, pl.ds(g * gs, gs), h].astype(F32).reshape(span, sw)
+                v = rows[h, i, pl.ds(g * gs, gs)].astype(F32).reshape(span, sw)
                 acc = acc + jnp.sum(v * v, axis=1, keepdims=True)
                 xn[h, at, i * sw:(i + 1) * sw] = (v * moe_gain[:, lo:lo + sw]).astype(BF16)
             ssq[at, :] = acc if h == 0 else ssq[at, :] + acc
@@ -446,30 +437,32 @@
     chunk = nx * cap
 
     def copy_e1(plane, yy):
-        return remote(e_p.at[plane, yy], e_r.at[plane, yy], se1.at[plane, yy], re1.at[plane, yy], {"tp": q})
+        return remote(e_p.at[plane, yy], e_r.at[plane, yy], se1, re1.at[plane, yy], {"tp": q})
 
     def copy_e2(plane, dy, h):
         ty = lax.rem(y + dy, ys)
         return remote(
-            es.at[plane, ty, h], er.at[plane, y, h], se2.at[plane, dy, h], re2.at[plane, dy, h],
+            es.at[plane, ty, h], er.at[plane, y, h], se2, re2.at[plane, dy - 1, h],
             {"tp": ty * 2 + core},
         )
 
     def copy_e3(peer, h):
-        return remote(outb.at[peer, h], ret.at[e, h], se3.at[peer, h], re3.at[e, h], {"ep": peer})
-
-    def landed_e3(src, h):
-        return remote(outb.at[src, h], ret.at[src, h], se3.at[src, h], re3.at[src, h], {"ep": src})
-
-    def issue(plane):
-        mine = hid[pl.ds(pl.multiple_of(plane * chunk, chunk), chunk), :]
-        for dy in list(range(1, ys)) + [0]:
+        return remote(outb.at[h, peer], ret.at[h, e], se3, re3.at[h], {"ep": peer})
+
+    def issue(planes, dys):
+        mine = jnp.concatenate([hid[pl.ds(pl.multiple_of(k * chunk, chunk), chunk), :] for k in planes], axis=0)
+        for dy in dys:
             ty = lax.rem(y + dy, ys)
             for h in range(HALVES):
-                e_p[plane, ty, h] = dot(mine, wed[:, block(ty * 2 + 1 - core, h)]).astype(BF16)
-            copy_e1(plane, ty).start()
+                value = dot(mine, wed[:, block(ty * 2 + 1 - core, h)]).astype(BF16)
+                for i, k in enumerate(planes):
+                    e_p[k, ty, h] = value[i * chunk:(i + 1) * chunk]
+            for k in planes:
+                copy_e1(k, ty).start()
             for h in range(HALVES):
-                e_o[plane, ty, h] = dot(mine, wed[:, block(ty * 2 + core, h)])
+                value = dot(mine, wed[:, block(ty * 2 + core, h)])
+                for i, k in enumerate(planes):
+                    e_o[k, ty, h] = value[i * chunk:(i + 1) * chunk]
 
     def push(plane):
         for dy in range(1, ys):
@@ -487,23 +480,17 @@
                 copy_e2(plane, dy, h).wait_recv()
                 result = result + er[plane, lax.rem(y - dy + ys, ys), h].astype(F32)
             result = result.reshape(nx, cap, sw).astype(BF16)
-            for i in range(nx):
-                outb[plane * nx + i, h] = result[i]
+            outb[h, pl.ds(plane * nx, nx)] = result
             for dx in range(first, nx):
                 copy_e3(peer_of(plane, dx), h).start()
 
-    @pl.loop(0, nz - 1)
-    def _(j):
-        issue(far(j))
-
-        @pl.when(j > 0)
-        def _():
-            push(far(j - 1))
-
-    issue(z)
-    if nz > 1:
-        push(far(nz - 2))
-    push(z)
+    order = [far(j) for j in range(nz - 1)] + [z]
+    pairs = [order[i:i + 2] for i in range(0, nz, 2)]
+    for planes in pairs:
+        issue(planes, range(1, ys))
+        issue(planes, [0])
+        for plane in planes:
+            push(plane)
 
     @pl.loop(0, nz - 1)
     def _(j):
@@ -511,62 +498,36 @@
 
     deliver(z, 1)
     for h in range(HALVES):
-        ret[e, h] = outb[e, h]
+        ret[h, e] = outb[h, e]
 
     def combine(weights, back):
         return lax.dot_general(weights, back, (((0,), (0,)), ((), ())), preferred_element_type=F32)
 
     for h in range(HALVES):
-        @pl.loop(1, n)
-        def _(d):
-            landed_e3(lax.rem(e + d, n), h).wait_recv()
-
-        back = jnp.concatenate([ret[i, h] for i in range(n)], axis=0)
+        others = ret.at[h, pl.ds(0, n - 1)]
+        remote(others, others, se3, re3.at[h], {"ep": peer_of(z, 1)}).wait_recv()
+        back = ret[h].astype(F32).reshape(slots, sw).astype(BF16)
         layer_v[:, h * sw:(h + 1) * sw] = (
             mixed[h] + combine(comb_hi, back) + combine(comb_lo, back)
         ).astype(BF16)
 
     puts[2].start()
 
-    @pl.loop(1, n)
-    def _(d):
-        peer = lax.rem(e + d, n)
-        copy_a(peer).wait_send()
-        copy_a2(peer).wait_send()
-        for h in range(HALVES):
-            copy_c1(peer, h).wait_send()
-            copy_e3(peer, h).wait_send()
-
-    @pl.loop(0, n)
-    def _(src):
-        for h in range(HALVES):
-            for dy in range(1, ys):
-                copy_c2(dy, src, h).wait_send()
-            for dy in range(ys):
-                copy_c3(dy, src, h).wait_send()
-
-    for dy in range(ys):
-        for h in range(HALVES):
-            copy_d1(dy, h).wait_send()
-            if dy:
-                copy_d2(dy, h).wait_send()
-
-    @pl.loop(0, nz)
-    def _(plane):
-        for yy in range(ys):
-            copy_e1(plane, yy).wait_send()
-        for dy in range(1, ys):
-            for h in range(HALVES):
-                copy_e2(plane, dy, h).wait_send()
-        for c in range(nc):
-            for dx in range(1, nx):
-                copy_x(plane, dx, c).wait_send()
-
-    @pl.loop(0, nz - 1)
-    def _(j):
-        plane = far(j)
-        for c in range(nc):
-            copy_z((plane < z).astype(jnp.int32), plane, c).wait_send()
+    def drain(ref, sem):
+        remote(ref, ref, sem, ra.at[0], {"tp": q}).wait_send()
+
+    drain(normed.at[pl.ds(0, n - 1), half], sa)
+    drain(cols.at[pl.ds(0, n - 1), half], sa2)
+    drain(part.at[:, pl.ds(0, nx - 1)], sb)
+    drain(zsend.at[pl.ds(0, nz - 1)], sz)
+    drain(op_p, sd1)
+    drain(hs.at[pl.ds(0, ys - 1)], sd2)
+    drain(sd.at[:, pl.ds(0, n - 1)], sc1)
+    drain(rows.at[:, pl.ds(0, ys - 1)], sc2)
+    drain(rows.at[:, pl.ds(0, ys)], sc3)
+    drain(e_p, se1)
+    drain(es.at[:, pl.ds(0, ys - 1)], se2)
+    drain(outb.at[:, pl.ds(0, n - 1)], se3)
 
     for put in puts:
         put.wait()
@@ -616,17 +577,17 @@
         V((g, chans), BF16), V((p, nh, g, sw), F32),
         V((ys, nh, g, sw), BF16), V((ys, nh, g, sw), F32), V((ys, nh, g, sw), BF16),
         V((ys, nh, g, sw), BF16), V((ys, nh, g, sw), BF16), V((nh, g, sw), F32),
-        V((n, nh, cap, sw), BF16), V((p, n, nh, cap, sw), BF16), V((nh, slots, p * sw), BF16), V((slots, 1), F32),
+        V((nh, n, cap, sw), BF16), V((nh, p, n, cap, sw), BF16), V((nh, slots, p * sw), BF16), V((slots, 1), F32),
         V((2, slots, hidden), F32), V((slots, hidden), BF16),
         V((nz, ys, nh, chunk, sw), BF16), V((nz, ys, nh, chunk, sw), F32), V((nz, ys, nh, chunk, sw), BF16),
         V((nz, ys, nh, chunk, sw), BF16), V((nz, ys, nh, chunk, sw), BF16),
-        V((n, nh, cap, sw), BF16), V((n, nh, cap, sw), BF16),
+        V((nh, n, cap, sw), BF16), V((nh, n, cap, sw), BF16),
         dma((8,)), dma((len(small),)), dma((3,)),
-        dma((n,)), dma((n,)), dma((n,)), dma((n,)),
-        dma((nz, nx, nc)), dma((nz, nx, nc)), dma((nz, nc)), dma((2, nz, nc)),
-        dma((ys, nh)), dma((ys, nh)), dma((ys, nh)), dma((ys, nh)),
-        dma((n, nh)), dma((n, nh)), dma((ys, n, nh)), dma((ys, n, nh)), dma((ys, n, nh)), dma((ys, n, nh)),
-        dma((nz, ys)), dma((nz, ys)), dma((nz, ys, nh)), dma((nz, ys, nh)), dma((n, nh)), dma((n, nh)),
+        dma, dma((n,)), dma, dma((n,)),
+        dma, dma((nz, nx - 1, nc)), dma, dma((2, nz, nc)),
+        dma, dma((ys, nh)), dma, dma((ys - 1, nh)),
+        dma, dma((n, nh)), dma, dma((ys - 1, n, nh)), dma, dma((nh,)),
+        dma, dma((nz, ys)), dma, dma((nz, ys - 1, nh)), dma, dma((nh,)),
     ]
     outs = (
         jax.ShapeDtypeStruct((g, share), BF16),

time: 91 us -> 85.8 us (0.943)
  Pallas kernels: 90.2 us -> 85 us
    pallas_call x1, Pallas kernels: 88.2 us -> 82.9 us  [shards(): pl.pallas_call(functools.partial(kernel, n, p, nx, cap), out_shape=outs,...]
where the time goes in v3:
time: 85.8 us; the launch traced here: 85.6 us
  Pallas kernels  85 us (99%)
    pallas_call x1, Pallas kernels, shards(): pl.pallas_call(functools.partial(kernel, n, p, nx, cap), out_shape=outs,...  82.9 us
    pallas_call x1, Pallas kernels, shards(): pl.pallas_call(finish, out_shape=outs, in_specs=[vm] * 3, out_specs=(vm,...  2.03 us

profile of v3, /device:TPU:0, one launch (start us, length us, event | category | flops | bytes accessed | tf_op | source)
XLA Modules:
  0.0 85.6 jit_solution(6181891256002852565)
XLA Ops:
  0.6 82.9 %shard_map.184 = (bf16[64,1024]{1,0:T(8,128)(2,1)}, f32[64,1024]{1,0:T(8,128)}, bf16[3,64,1024]{2,1,0:T(8,128)(2,1)}) custom-call(bf16[64,4096]{1,0:T(8,128)(2,1)} %tokens_h.1, f32[64,1024]{1,0:T(8,128)} %state_h.1, bf16[3,64,1024]{2,1,0:T(8,128)(2,1)} %bitcast.7, bf16[32,128]{1,0:T(8,128)(2,1)} %bitcast.8, bf16[32,128]{1,0:T(8,128)(2,1)} %bitcast.9, ...), custom_call_target="tpu_custom_call" | custom-call | tf_op jit(solution)/shard_map/pallas_call | solution.py:597
  83.6 2.0 %shard_map.185 = (bf16[64,1024]{1,0:T(8,128)(2,1)}, f32[64,1024]{1,0:T(8,128)}, bf16[3,64,1024]{2,1,0:T(8,128)(2,1)}) custom-call(bf16[64,1024]{1,0:T(8,128)(2,1)} %get-tuple-element.9.layer_in, f32[64,1024]{1,0:T(8,128)} %get-tuple-element.10.state_in, bf16[3,64,1024]{2,1,0:T(8,128)(2,1)} %get-tuple-element.11.conv_in), custom_call_target="tpu_custom_call" | custom-call | tf_op jit(solution)/shard_map/pallas_call | solution.py:610

commit v4 on v3

--- a/solution.py
+++ b/solution.py
@@ -11,7 +11,7 @@
 F32 = jnp.float32
 BF16 = jnp.bfloat16
 HALVES = 2
-LAG = 3
+LAG = 5
 
 
 def dot(a, b):
@@ -32,10 +32,10 @@
     tokens, state_in, conv_in, mix_gain_in, moe_gain_in, conv_w, rate_param, routes, prob,
     layer_v, state_v, conv_v,
     wr, wg, wrate, winput, wout, weg, weu, wed,
-    mix_gain, moe_gain, normed, cols, part, bx, zsend, rz, gated, oacc,
+    mix_gain, moe_gain, normed, cols, part, bx, zsend, rz, zf, gated, oacc,
     op_p, op_o, op_r, hs, hr, mixed,
     sd, rows, xn, ssq, gacc, hid, e_p, e_o, e_r, es, er, outb, ret,
-    wsem, lsem, osem, sa, ra, sa2, ra2, sb, rb, sz, rzs, sd1, rd1, sd2, rd2,
+    wsem, lsem, osem, sa, ra, sa2, ra2, sb, rb, sz, rzs, szf, rzf, sd1, rd1, sd2, rd2,
     sc1, rc1, sc2, rc2, sc3, rc3, se1, re1, se2, re2, se3, re3,
 ):
     e = lax.axis_index("ep")
@@ -94,6 +94,17 @@
 
     small[0].wait()
     small[1].wait()
+    nc, bw = rate_h.shape[0], rate_h.shape[1]
+    late = nc // 2
+    paired = nz % 2 == 0 and nz > 2
+    middle = (z == nz // 2) | (z == nz // 2 - 1)
+    opposite = nz - 1 - z
+    if paired:
+        @pl.when(middle)
+        def _():
+            for dx in range(1, nx):
+                bx[opposite, dx, late:] = jnp.zeros((nc - late,) + bx.shape[3:], BF16)
+
     for j in range(width // 128):
         cs = slice(j * 128, (j + 1) * 128)
         mix_gain[:, cs] = mix_gain_in[j:j + 1, :].astype(F32)
@@ -110,15 +121,23 @@
     pl.semaphore_wait(barrier, n + p - 2)
 
     half = pl.ds(pl.multiple_of(core * (rows_g // 2), rows_g // 2), rows_g // 2)
-    nc, bw = rate_h.shape[0], rate_h.shape[1]
     high = (2 * z) // nz
     folded = z + high * (nz - 1 - 2 * z)
 
-    def far(j):
+    lead = nz - 1 - 2 * folded
+
+    def across(j):
         plane = nz - 1 - j
         plane = plane - (folded >= plane).astype(jnp.int32)
         return plane + high * (nz - 1 - 2 * plane)
 
+    def far(j):
+        ahead = (j < lead).astype(jnp.int32)
+        k = (1 - ahead) * (j - lead)
+        turn = folded + (folded - k // 2) * (2 * lax.rem(k, 2) - 1)
+        plane = ahead * (nz - 1 - j) + (1 - ahead) * turn
+        return plane + high * (nz - 1 - 2 * plane)
+
     def beside(dx):
         return lax.rem(x + dx, nx)
 
@@ -140,7 +159,7 @@
     @pl.loop(0, nz - 1)
     def _(j):
         for dx in range(nx):
-            copy_a(peer_of(far(j), dx)).start()
+            copy_a(peer_of(across(j), dx)).start()
 
     cols[e] = normed[e]
 
@@ -183,6 +202,21 @@
             {"ep": peer_of(z, dx)},
         )
 
+    def copy_f(dx, c):
+        return remote(
+            part.at[opposite, beside(dx), c], zf.at[dx - 1, c - late], szf, rzf.at[dx - 1, c - late],
+            {"ep": opposite * nx + x},
+        )
+
+    def by_line(plane, c):
+        return middle & (plane == opposite) if paired and c >= late else None
+
+    def unless(flag, action):
+        if flag is None:
+            action()
+        else:
+            pl.when(jnp.logical_not(flag))(action)
+
     def project(plane, last, own):
         first = 1 if own else 0
         for dx in range(first, nx):
@@ -199,18 +233,29 @@
                 for i in range(nx):
                     part[plane, i, c, :, lo:lo + bw] = value[i * rows_g:(i + 1) * rows_g]
             if c < last:
+                flag = None if own else by_line(plane, c)
                 for dx in range(1, nx):
-                    copy_x(plane, dx, c).start()
-
-    project(z, nc // 2, True)
+                    unless(flag, copy_x(plane, dx, c).start)
+                    if flag is not None:
+                        pl.when(flag)(copy_f(dx, c).start)
+
+    project(z, late, True)
 
     @pl.loop(0, nz - 1)
     def _(j):
         project(far(j), nc, False)
 
-    for c in range(nc // 2, nc):
-        for dx in range(1, nx):
-            copy_x(z, dx, c).start()
+    def rest_of_own():
+        for c in range(late, nc):
+            for dx in range(1, nx):
+                if paired:
+                    @pl.when(middle)
+                    def _():
+                        copy_f(dx, c).wait_recv()
+                        mine = part[z, beside(dx), c].astype(F32)
+                        part[z, beside(dx), c] = (mine + zf[dx - 1, c - late].astype(F32)).astype(BF16)
+
+                copy_x(z, dx, c).start()
 
     def copy_z(side, plane, c):
         to = z + 1 - 2 * side
@@ -221,7 +266,7 @@
 
     def summed(sides, plane, c):
         for dx in range(1, nx):
-            copy_x(plane, dx, c).wait_recv()
+            unless(by_line(plane, c) if len(sides) == 1 else None, copy_x(plane, dx, c).wait_recv)
         total = part[plane, x, c].astype(F32)
         for dx in range(1, nx):
             total = total + bx[plane, dx, c].astype(F32)
@@ -235,13 +280,18 @@
             total = total + rz[s, plane, c].astype(F32)
         return total
 
-    @pl.loop(0, nz - 1)
-    def _(j):
+    def line_step(j):
         plane = far(j)
         side = (plane < z).astype(jnp.int32)
         for c in range(nc):
             zsend[plane, c] = summed([side], plane, c).astype(BF16)
             copy_z(side, plane, c).start()
+
+    if nz > 1:
+        line_step(jnp.int32(0))
+    rest_of_own()
+    if nz > 1:
+        pl.loop(1, nz - 1)(line_step)
 
     def block(i, h):
         return pl.ds(pl.multiple_of(i * share + h * sw, sw), sw)
@@ -291,15 +341,17 @@
         ty = lax.rem(y + dy, ys)
         return remote(hs.at[ty, h], hr.at[y, h], sd2, rd2.at[dy - 1, h], {"tp": ty * 2 + core})
 
-    for dy in range(ys):
-        yy = lax.rem(y + dy + 1, ys)
-        for h in range(HALVES):
-            op_p[yy, h] = out_part(yy * 2 + 1 - core, h).astype(BF16)
-            copy_d1(yy, h).start()
-    for dy in range(ys):
-        yy = lax.rem(y + dy + 1, ys)
-        for h in range(HALVES):
-            op_o[yy, h] = out_part(yy * 2 + core, h)
+    def out_parts(dys):
+        for yy in [lax.rem(y + dy, ys) for dy in dys]:
+            for h in range(HALVES):
+                op_p[yy, h] = out_part(yy * 2 + 1 - core, h).astype(BF16)
+                copy_d1(yy, h).start()
+        for yy in [lax.rem(y + dy, ys) for dy in dys]:
+            for h in range(HALVES):
+                op_o[yy, h] = out_part(yy * 2 + core, h)
+
+    out_parts(range(1, ys))
+    out_parts([0])
     for h in range(HALVES):
         for dy in range(1, ys):
             ty = lax.rem(y + dy, ys)
@@ -351,7 +403,7 @@
         @pl.loop(0, nz - 1)
         def _(j):
             for dx in range(nx):
-                copy_c1(peer_of(far(nz - 2 - j), dx), h).start()
+                copy_c1(peer_of(across(j), dx), h).start()
 
         rows[h, t, e] = sd[h, e]
         for dy in range(1, ys):
@@ -400,28 +452,32 @@
         tasks.append(functools.partial(early, 0, weg, f))
         tasks.append(functools.partial(early, 1, weu, f))
 
-    near = [(z, dx) for dx in range(1, nx)]
-    near = near + [(far(j), dx) for j in reversed(range(nz - 1)) for dx in range(nx)]
-    steps = [(peer_of(plane, dx), h) for h in range(HALVES) for plane, dx in near]
+    groups = [[peer_of(z, dx) for dx in range(1, nx)]]
+    groups = groups + [[peer_of(across(j), dx) for dx in range(nx)] for j in reversed(range(nz - 1))]
+    steps = []
+    for k in range(nz + 1):
+        steps = steps + [(src, 0) for src in (groups[k] if k < nz else [])]
+        steps = steps + [(src, 1) for src in (groups[k - 1] if k else [])]
     queue = [(e, h) for h in range(HALVES)]
-    begin = len(near) + len(near) // 2
-    for i, (src, h) in enumerate(steps):
+
+    def pass_on():
+        src, h = queue.pop(0)
+        for dy in range(1, ys):
+            landed_c2(dy, src, h).wait_recv()
+            copy_c3(dy, src, h).start()
+
+    for src, h in steps:
         landed_c1(src, h).wait_recv()
         for dy in range(1, ys):
             copy_c2(dy, src, h).start()
         copy_c3(0, src, h).start()
         queue.append((src, h))
         if len(queue) > LAG:
-            was, wh = queue.pop(0)
-            for dy in range(1, ys):
-                landed_c2(dy, was, wh).wait_recv()
-                copy_c3(dy, was, wh).start()
-        if i >= begin and tasks:
+            pass_on()
+    while queue:
+        pass_on()
+        if tasks:
             tasks.pop(0)()
-    for was, wh in queue:
-        for dy in range(1, ys):
-            landed_c2(dy, was, wh).wait_recv()
-            copy_c3(dy, was, wh).start()
     for task in tasks:
         task()
 
@@ -436,8 +492,8 @@
     loads[7].wait()
     chunk = nx * cap
 
-    def copy_e1(plane, yy):
-        return remote(e_p.at[plane, yy], e_r.at[plane, yy], se1, re1.at[plane, yy], {"tp": q})
+    def copy_e1(plane, yy, h):
+        return remote(e_p.at[plane, yy, h], e_r.at[plane, yy, h], se1, re1.at[plane, yy, h], {"tp": q})
 
     def copy_e2(plane, dy, h):
         ty = lax.rem(y + dy, ys)
@@ -457,8 +513,7 @@
                 value = dot(mine, wed[:, block(ty * 2 + 1 - core, h)]).astype(BF16)
                 for i, k in enumerate(planes):
                     e_p[k, ty, h] = value[i * chunk:(i + 1) * chunk]
-            for k in planes:
-                copy_e1(k, ty).start()
+                    copy_e1(k, ty, h).start()
             for h in range(HALVES):
                 value = dot(mine, wed[:, block(ty * 2 + core, h)])
                 for i, k in enumerate(planes):
@@ -467,14 +522,14 @@
     def push(plane):
         for dy in range(1, ys):
             ty = lax.rem(y + dy, ys)
-            copy_e1(plane, ty).wait_recv()
             for h in range(HALVES):
+                copy_e1(plane, ty, h).wait_recv()
                 es[plane, ty, h] = (e_o[plane, ty, h] + e_r[plane, ty, h].astype(F32)).astype(BF16)
                 copy_e2(plane, dy, h).start()
 
     def deliver(plane, first):
-        copy_e1(plane, y).wait_recv()
         for h in range(HALVES):
+            copy_e1(plane, y, h).wait_recv()
             result = e_o[plane, y, h] + e_r[plane, y, h].astype(F32)
             for dy in range(1, ys):
                 copy_e2(plane, dy, h).wait_recv()
@@ -484,7 +539,7 @@
             for dx in range(first, nx):
                 copy_e3(peer_of(plane, dx), h).start()
 
-    order = [far(j) for j in range(nz - 1)] + [z]
+    order = [across(j) for j in range(nz - 1)] + [z]
     pairs = [order[i:i + 2] for i in range(0, nz, 2)]
     for planes in pairs:
         issue(planes, range(1, ys))
@@ -494,7 +549,7 @@
 
     @pl.loop(0, nz - 1)
     def _(j):
-        deliver(far(j), 0)
+        deliver(across(j), 0)
 
     deliver(z, 1)
     for h in range(HALVES):
@@ -518,7 +573,18 @@
 
     drain(normed.at[pl.ds(0, n - 1), half], sa)
     drain(cols.at[pl.ds(0, n - 1), half], sa2)
-    drain(part.at[:, pl.ds(0, nx - 1)], sb)
+    if paired:
+        @pl.when(middle)
+        def _():
+            drain(part.at[pl.ds(0, nz - 1), pl.ds(0, nx - 1)], sb)
+            drain(part.at[0, pl.ds(0, nx - 1), pl.ds(0, late)], sb)
+            drain(zf, szf)
+
+        @pl.when(jnp.logical_not(middle))
+        def _():
+            drain(part.at[:, pl.ds(0, nx - 1)], sb)
+    else:
+        drain(part.at[:, pl.ds(0, nx - 1)], sb)
     drain(zsend.at[pl.ds(0, nz - 1)], sz)
     drain(op_p, sd1)
     drain(hs.at[pl.ds(0, ys - 1)], sd2)
@@ -573,7 +639,7 @@
         V((1, width), F32), V((1, width), F32),
         V((n, g, depth), BF16), V((n, g, depth), BF16),
         V((nz, nx, nc, g, cw), BF16), V((nz, nx, nc, g, cw), BF16),
-        V((nz, nc, g, cw), BF16), V((2, nz, nc, g, cw), BF16),
+        V((nz, nc, g, cw), BF16), V((2, nz, nc, g, cw), BF16), V((nx - 1, nc - nc // 2, g, cw), BF16),
         V((g, chans), BF16), V((p, nh, g, sw), F32),
         V((ys, nh, g, sw), BF16), V((ys, nh, g, sw), F32), V((ys, nh, g, sw), BF16),
         V((ys, nh, g, sw), BF16), V((ys, nh, g, sw), BF16), V((nh, g, sw), F32),
@@ -584,10 +650,10 @@
         V((nh, n, cap, sw), BF16), V((nh, n, cap, sw), BF16),
         dma((8,)), dma((len(small),)), dma((3,)),
         dma, dma((n,)), dma, dma((n,)),
-        dma, dma((nz, nx - 1, nc)), dma, dma((2, nz, nc)),
+        dma, dma((nz, nx - 1, nc)), dma, dma((2, nz, nc)), dma, dma((nx - 1, nc - nc // 2)),
         dma, dma((ys, nh)), dma, dma((ys - 1, nh)),
         dma, dma((n, nh)), dma, dma((ys - 1, n, nh)), dma, dma((nh,)),
-        dma, dma((nz, ys)), dma, dma((nz, ys - 1, nh)), dma, dma((nh,)),
+        dma, dma((nz, ys, nh)), dma, dma((nz, ys - 1, nh)), dma, dma((nh,)),
     ]
     outs = (
         jax.ShapeDtypeStruct((g, share), BF16),

time: 85.8 us -> 85.2 us (level)
  no operation moved by 1% of the time
where the time goes in v4:
time: 85.2 us; the launch traced here: 85.1 us
  Pallas kernels  84.4 us (99%)
    pallas_call x1, Pallas kernels, shards(): pl.pallas_call(functools.partial(kernel, n, p, nx, cap), out_shape=outs,...  82.4 us
    pallas_call x1, Pallas kernels, shards(): pl.pallas_call(finish, out_shape=outs, in_specs=[vm] * 3, out_specs=(vm,...  2.03 us

profile of v4, /device:TPU:0, one launch (start us, length us, event | category | flops | bytes accessed | tf_op | source)
XLA Modules:
  0.0 85.1 jit_solution(10202408497133112301)
XLA Ops:
  0.6 82.4 %shard_map.184 = (bf16[64,1024]{1,0:T(8,128)(2,1)}, f32[64,1024]{1,0:T(8,128)}, bf16[3,64,1024]{2,1,0:T(8,128)(2,1)}) custom-call(bf16[64,4096]{1,0:T(8,128)(2,1)} %tokens_h.1, f32[64,1024]{1,0:T(8,128)} %state_h.1, bf16[3,64,1024]{2,1,0:T(8,128)(2,1)} %bitcast.7, bf16[32,128]{1,0:T(8,128)(2,1)} %bitcast.8, bf16[32,128]{1,0:T(8,128)(2,1)} %bitcast.9, ...), custom_call_target="tpu_custom_call" | custom-call | tf_op jit(solution)/shard_map/pallas_call | solution.py:663
  83.0 2.0 %shard_map.185 = (bf16[64,1024]{1,0:T(8,128)(2,1)}, f32[64,1024]{1,0:T(8,128)}, bf16[3,64,1024]{2,1,0:T(8,128)(2,1)}) custom-call(bf16[64,1024]{1,0:T(8,128)(2,1)} %get-tuple-element.9.layer_in, f32[64,1024]{1,0:T(8,128)} %get-tuple-element.10.state_in, bf16[3,64,1024]{2,1,0:T(8,128)(2,1)} %get-tuple-element.11.conv_in), custom_call_target="tpu_custom_call" | custom-call | tf_op jit(solution)/shard_map/pallas_call | solution.py:676

commit v5 on v4

--- a/solution.py
+++ b/solution.py
@@ -11,7 +11,6 @@
 F32 = jnp.float32
 BF16 = jnp.bfloat16
 HALVES = 2
-LAG = 5
 
 
 def dot(a, b):
@@ -34,9 +33,9 @@
     wr, wg, wrate, winput, wout, weg, weu, wed,
     mix_gain, moe_gain, normed, cols, part, bx, zsend, rz, zf, gated, oacc,
     op_p, op_o, op_r, hs, hr, mixed,
-    sd, rows, xn, ssq, gacc, hid, e_p, e_o, e_r, es, er, outb, ret,
+    mb, ag, sdo, sd, rows, xn, ssq, gacc, hid, e_p, e_o, e_r, es, er, outb, ret,
     wsem, lsem, osem, sa, ra, sa2, ra2, sb, rb, sz, rzs, szf, rzf, sd1, rd1, sd2, rd2,
-    sc1, rc1, sc2, rc2, sc3, rc3, se1, re1, se2, re2, se3, re3,
+    sag, rag, sco, sc1, rc1, sc2, rc2, sc3, rc3, se1, re1, se2, re2, ro2, se3, re3,
 ):
     e = lax.axis_index("ep")
     t = lax.axis_index("tp")
@@ -145,13 +144,14 @@
         return plane * nx + beside(dx)
 
     def copy_a(peer):
-        return remote(normed.at[peer, half], cols.at[e, half], sa, ra.at[e], {"ep": peer})
-
-    def landed_a(src):
-        return remote(normed.at[src, half], cols.at[src, half], sa, ra.at[src], {"ep": src})
-
-    def copy_a2(src):
-        return remote(cols.at[src, half], cols.at[src, half], sa2, ra2.at[src], {"tp": q})
+        return remote(normed.at[peer, half], cols.at[e, half], sa, ra.at[z], {"ep": peer})
+
+    def copy_a2(src, plane):
+        return remote(cols.at[src, half], cols.at[src, half], sa2, ra2.at[plane], {"tp": q})
+
+    def landed(plane, count, sem):
+        block = cols.at[pl.ds(0, count), half]
+        remote(block, block, sa, sem.at[plane], {"tp": q}).wait_recv()
 
     for dx in range(1, nx):
         copy_a(peer_of(z, dx)).start()
@@ -219,12 +219,11 @@
 
     def project(plane, last, own):
         first = 1 if own else 0
-        for dx in range(first, nx):
-            src = peer_of(plane, dx)
-            landed_a(src).wait_recv()
-            copy_a2(src).start()
-        for dx in range(first, nx):
-            copy_a2(peer_of(plane, dx)).wait_recv()
+        if nx > first:
+            landed(plane, nx - first, ra)
+            for dx in range(first, nx):
+                copy_a2(peer_of(plane, dx), plane).start()
+            landed(plane, nx - first, ra2)
         feats = cols[pl.ds(plane * nx, nx)].reshape(nx * rows_g, depth)
         for c in range(nc):
             cs = slice(c * bw, (c + 1) * bw)
@@ -257,10 +256,11 @@
 
                 copy_x(z, dx, c).start()
 
-    def copy_z(side, plane, c):
+    def copy_z(side, plane, c, at=None):
         to = z + 1 - 2 * side
+        slot = plane + side * ((to if at is None else at) == plane).astype(jnp.int32) * (nz - plane)
         return remote(
-            zsend.at[plane, c], rz.at[side, plane, c], sz, rzs.at[side, plane, c],
+            zsend.at[plane, c], rz.at[side, plane, c], sz, rzs.at[slot, c],
             {"ep": to * nx + x},
         )
 
@@ -275,7 +275,7 @@
 
             @pl.when((origin >= 0) & (origin < nz))
             def _():
-                copy_z(s, plane, c).wait_recv()
+                copy_z(s, plane, c, z).wait_recv()
 
             total = total + rz[s, plane, c].astype(F32)
         return total
@@ -388,6 +388,23 @@
             rows.at[h, held, src], rows.at[h, held, src], sc3, rc3.at[h], {"tp": q}
         )
 
+    def copy_g(dy, h):
+        ty = lax.rem(y + dy, ys)
+        return remote(mb.at[h], ag.at[y, h], sag, rag.at[dy - 1, h], {"tp": ty * 2 + core})
+
+    def copy_o(dy, peer, h):
+        held = lax.rem(y - dy + ys, ys) * 2 + core
+        return remote(sdo.at[dy - 1, h, peer], rows.at[h, held, e], sco, rc2.at[dy - 1, e, h], {"ep": peer})
+
+    def landed_o(dy, src, h):
+        held = lax.rem(y - dy + ys, ys) * 2 + core
+        return remote(sdo.at[dy - 1, h, src], rows.at[h, held, src], sco, rc2.at[dy - 1, src, h], {"ep": src})
+
+    ncross = nz // 2 if nz % 2 == 0 else nz - 1
+    beyond = [[peer_of(across(j), dx) for dx in range(nx)] for j in reversed(range(ncross))]
+    near = [peer_of(z, dx) for dx in range(1, nx)]
+    near = near + [peer_of(across(j), dx) for j in range(ncross, nz - 1) for dx in range(nx)]
+
     for h in range(HALVES):
         copy_d1(y, h).wait_recv()
         total = tokens[:, block(t, h)].astype(F32) + op_o[y, h] + op_r[y, h].astype(F32)
@@ -395,19 +412,19 @@
             copy_d2(dy, h).wait_recv()
             total = total + hr[lax.rem(y - dy + ys, ys), h].astype(F32)
         mixed[h] = total
-        sent = dot(dispatch, total.astype(BF16)).reshape(n, cap, sw).astype(BF16)
-        sd[h] = sent
-        for dx in range(1, nx):
-            copy_c1(peer_of(z, dx), h).start()
-
-        @pl.loop(0, nz - 1)
+        mb[h] = total.astype(BF16)
+        for dy in range(1, ys):
+            copy_g(dy, h).start()
+        sd[h] = dot(dispatch, mb[h]).reshape(n, cap, sw).astype(BF16)
+
+        @pl.loop(0, ncross)
         def _(j):
             for dx in range(nx):
                 copy_c1(peer_of(across(j), dx), h).start()
 
+        for peer in near:
+            copy_c1(peer, h).start()
         rows[h, t, e] = sd[h, e]
-        for dy in range(1, ys):
-            copy_c2(dy, e, h).start()
         copy_c3(0, e, h).start()
 
     gs = min(n, max(1, 64 // cap))
@@ -452,32 +469,66 @@
         tasks.append(functools.partial(early, 0, weg, f))
         tasks.append(functools.partial(early, 1, weu, f))
 
-    groups = [[peer_of(z, dx) for dx in range(1, nx)]]
-    groups = groups + [[peer_of(across(j), dx) for dx in range(nx)] for j in reversed(range(nz - 1))]
-    steps = []
-    for k in range(nz + 1):
-        steps = steps + [(src, 0) for src in (groups[k] if k < nz else [])]
-        steps = steps + [(src, 1) for src in (groups[k - 1] if k else [])]
-    queue = [(e, h) for h in range(HALVES)]
-
-    def pass_on():
-        src, h = queue.pop(0)
+    def gathered(h):
+        for dy in range(1, ys):
+            origin = lax.rem(y - dy + ys, ys)
+            copy_g(dy, h).wait_recv()
+            sdo[dy - 1, h] = dot(dispatch, ag[origin, h]).reshape(n, cap, sw).astype(BF16)
+            for peer in near:
+                copy_o(dy, peer, h).start()
+            rows[h, origin * 2 + core, e] = sdo[dy - 1, h, e]
+            copy_c3(dy, e, h).start()
+
+    def near_own(src, h):
+        landed_c1(src, h).wait_recv()
+        copy_c3(0, src, h).start()
+
+    def near_other(src, h):
+        for dy in range(1, ys):
+            landed_o(dy, src, h).wait_recv()
+            copy_c3(dy, src, h).start()
+
+    def pass_on(src, h):
         for dy in range(1, ys):
             landed_c2(dy, src, h).wait_recv()
             copy_c3(dy, src, h).start()
 
-    for src, h in steps:
+    def cross(src, h):
         landed_c1(src, h).wait_recv()
         for dy in range(1, ys):
             copy_c2(dy, src, h).start()
         copy_c3(0, src, h).start()
-        queue.append((src, h))
-        if len(queue) > LAG:
-            pass_on()
-    while queue:
-        pass_on()
-        if tasks:
-            tasks.pop(0)()
+
+    gathered(0)
+    for h in range(HALVES):
+        for i, group in enumerate(beyond):
+            for src in group:
+                cross(src, h)
+            if h == 0 and i == 0:
+                gathered(1)
+            if h and i == 0:
+                for src in near:
+                    near_own(src, 0)
+                    near_other(src, 0)
+        if h == 0:
+            for group in beyond[:-1]:
+                for src in group:
+                    pass_on(src, 0)
+    for src in beyond[-1] if beyond else []:
+        pass_on(src, 0)
+    if not beyond:
+        gathered(1)
+        for src in near:
+            near_own(src, 0)
+            near_other(src, 0)
+    rest = [functools.partial(near_own, src, 1) for src in near]
+    rest = rest + [functools.partial(near_other, src, 1) for src in near]
+    for step in rest:
+        step()
+    rest = [functools.partial(pass_on, src, 1) for group in beyond for src in group]
+    while rest:
+        tasks.pop(0)() if tasks else None
+        rest.pop(0)()
     for task in tasks:
         task()
 
@@ -501,6 +552,18 @@
             es.at[plane, ty, h], er.at[plane, y, h], se2, re2.at[plane, dy - 1, h],
             {"tp": ty * 2 + core},
         )
+
+    def mine_of(dx):
+        return pl.ds(pl.multiple_of(beside(dx) * cap, cap), cap)
+
+    def copy_own(dy, dx, h):
+        ty = lax.rem(y + dy, ys)
+        return remote(
+            es.at[z, ty, h, mine_of(dx)], er.at[z, y, h, mine_of(dx)], se2, ro2.at[dy - 1, dx, h],
+            {"tp": ty * 2 + core},
+        )
+
+    own_order = [(dx, h) for dx in list(range(1, nx)) + [0] for h in range(HALVES)]
 
     def copy_e3(peer, h):
         return remote(outb.at[h, peer], ret.at[h, e], se3, re3.at[h], {"ep": peer})
@@ -527,7 +590,32 @@
                 es[plane, ty, h] = (e_o[plane, ty, h] + e_r[plane, ty, h].astype(F32)).astype(BF16)
                 copy_e2(plane, dy, h).start()
 
-    def deliver(plane, first):
+    def push_own():
+        for dy in range(1, ys):
+            ty = lax.rem(y + dy, ys)
+            for h in range(HALVES):
+                copy_e1(z, ty, h).wait_recv()
+            for dx, h in own_order:
+                at = mine_of(dx)
+                es[z, ty, h, at] = (e_o[z, ty, h, at] + e_r[z, ty, h, at].astype(F32)).astype(BF16)
+                copy_own(dy, dx, h).start()
+
+    def deliver_own():
+        for h in range(HALVES):
+            copy_e1(z, y, h).wait_recv()
+        for dx, h in own_order:
+            at = mine_of(dx)
+            result = e_o[z, y, h, at] + e_r[z, y, h, at].astype(F32)
+            for dy in range(1, ys):
+                copy_own(dy, dx, h).wait_recv()
+                result = result + er[z, lax.rem(y - dy + ys, ys), h, at].astype(F32)
+            if dx:
+                outb[h, peer_of(z, dx)] = result.astype(BF16)
+                copy_e3(peer_of(z, dx), h).start()
+            else:
+                ret[h, e] = result.astype(BF16)
+
+    def deliver(plane):
         for h in range(HALVES):
             copy_e1(plane, y, h).wait_recv()
             result = e_o[plane, y, h] + e_r[plane, y, h].astype(F32)
@@ -536,7 +624,7 @@
                 result = result + er[plane, lax.rem(y - dy + ys, ys), h].astype(F32)
             result = result.reshape(nx, cap, sw).astype(BF16)
             outb[h, pl.ds(plane * nx, nx)] = result
-            for dx in range(first, nx):
+            for dx in range(nx):
                 copy_e3(peer_of(plane, dx), h).start()
 
     order = [across(j) for j in range(nz - 1)] + [z]
@@ -545,15 +633,13 @@
         issue(planes, range(1, ys))
         issue(planes, [0])
         for plane in planes:
-            push(plane)
+            push_own() if plane is z else push(plane)
 
     @pl.loop(0, nz - 1)
     def _(j):
-        deliver(across(j), 0)
-
-    deliver(z, 1)
-    for h in range(HALVES):
-        ret[h, e] = outb[h, e]
+        deliver(across(j))
+
+    deliver_own()
 
     def combine(weights, back):
         return lax.dot_general(weights, back, (((0,), (0,)), ((), ())), preferred_element_type=F32)
@@ -589,7 +675,9 @@
     drain(op_p, sd1)
     drain(hs.at[pl.ds(0, ys - 1)], sd2)
     drain(sd.at[:, pl.ds(0, n - 1)], sc1)
-    drain(rows.at[:, pl.ds(0, ys - 1)], sc2)
+    drain(rows.at[:, pl.ds(0, ys - 1), pl.ds(0, n - 1 - len(near))], sc2)
+    drain(ag.at[pl.ds(0, ys - 1)], sag)
+    drain(sdo.at[:, :, pl.ds(0, len(near))], sco)
     drain(rows.at[:, pl.ds(0, ys)], sc3)
     drain(e_p, se1)
     drain(es.at[:, pl.ds(0, ys - 1)], se2)
@@ -643,17 +731,19 @@
         V((g, chans), BF16), V((p, nh, g, sw), F32),
         V((ys, nh, g, sw), BF16), V((ys, nh, g, sw), F32), V((ys, nh, g, sw), BF16),
         V((ys, nh, g, sw), BF16), V((ys, nh, g, sw), BF16), V((nh, g, sw), F32),
+        V((nh, g, sw), BF16), V((ys, nh, g, sw), BF16), V((ys - 1, nh, n, cap, sw), BF16),
         V((nh, n, cap, sw), BF16), V((nh, p, n, cap, sw), BF16), V((nh, slots, p * sw), BF16), V((slots, 1), F32),
         V((2, slots, hidden), F32), V((slots, hidden), BF16),
         V((nz, ys, nh, chunk, sw), BF16), V((nz, ys, nh, chunk, sw), F32), V((nz, ys, nh, chunk, sw), BF16),
         V((nz, ys, nh, chunk, sw), BF16), V((nz, ys, nh, chunk, sw), BF16),
         V((nh, n, cap, sw), BF16), V((nh, n, cap, sw), BF16),
         dma((8,)), dma((len(small),)), dma((3,)),
-        dma, dma((n,)), dma, dma((n,)),
-        dma, dma((nz, nx - 1, nc)), dma, dma((2, nz, nc)), dma, dma((nx - 1, nc - nc // 2)),
+        dma, dma((nz,)), dma, dma((nz,)),
+        dma, dma((nz, nx - 1, nc)), dma, dma((nz + 1, nc)), dma, dma((nx - 1, nc - nc // 2)),
         dma, dma((ys, nh)), dma, dma((ys - 1, nh)),
+        dma, dma((ys - 1, nh)), dma,
         dma, dma((n, nh)), dma, dma((ys - 1, n, nh)), dma, dma((nh,)),
-        dma, dma((nz, ys, nh)), dma, dma((nz, ys - 1, nh)), dma, dma((nh,)),
+        dma, dma((nz, ys, nh)), dma, dma((nz, ys - 1, nh)), dma((ys - 1, nx, nh)), dma, dma((nh,)),
     ]
     outs = (
         jax.ShapeDtypeStruct((g, share), BF16),

time: 85.2 us -> 84.2 us (0.988)
  Pallas kernels: 84.4 us -> 83.4 us
    pallas_call x1, Pallas kernels: 82.4 us -> 81.3 us  [shards(): pl.pallas_call(functools.partial(kernel, n, p, nx, cap), out_shape=outs,...]
where the time goes in v5:
time: 84.2 us; the launch traced here: 84 us
  Pallas kernels  83.4 us (99%)
    pallas_call x1, Pallas kernels, shards(): pl.pallas_call(functools.partial(kernel, n, p, nx, cap), out_shape=outs,...  81.3 us
    pallas_call x1, Pallas kernels, shards(): pl.pallas_call(finish, out_shape=outs, in_specs=[vm] * 3, out_specs=(vm,...  2.03 us

profile of v5, /device:TPU:0, one launch (start us, length us, event | category | flops | bytes accessed | tf_op | source)
XLA Modules:
  0.0 84.0 jit_solution(398946553025273234)
XLA Ops:
  0.6 81.3 %shard_map.184 = (bf16[64,1024]{1,0:T(8,128)(2,1)}, f32[64,1024]{1,0:T(8,128)}, bf16[3,64,1024]{2,1,0:T(8,128)(2,1)}) custom-call(bf16[64,4096]{1,0:T(8,128)(2,1)} %tokens_h.1, f32[64,1024]{1,0:T(8,128)} %state_h.1, bf16[3,64,1024]{2,1,0:T(8,128)(2,1)} %bitcast.7, bf16[32,128]{1,0:T(8,128)(2,1)} %bitcast.8, bf16[32,128]{1,0:T(8,128)(2,1)} %bitcast.9, ...), custom_call_target="tpu_custom_call" | custom-call | tf_op jit(solution)/shard_map/pallas_call | solution.py:753
  82.0 2.0 %shard_map.185 = (bf16[64,1024]{1,0:T(8,128)(2,1)}, f32[64,1024]{1,0:T(8,128)}, bf16[3,64,1024]{2,1,0:T(8,128)(2,1)}) custom-call(bf16[64,1024]{1,0:T(8,128)(2,1)} %get-tuple-element.9.layer_in, f32[64,1024]{1,0:T(8,128)} %get-tuple-element.10.state_in, bf16[3,64,1024]{2,1,0:T(8,128)(2,1)} %get-tuple-element.11.conv_in), custom_call_target="tpu_custom_call" | custom-call | tf_op jit(solution)/shard_map/pallas_call | solution.py:766

commit v6 on v5

--- a/solution.py
+++ b/solution.py
@@ -382,10 +382,10 @@
             rows.at[h, held, src], rows.at[h, held, src], sc2, rc2.at[dy - 1, src, h], {"tp": held}
         )
 
-    def copy_c3(dy, src, h):
+    def copy_c3(dy, src, h, away=0):
         held = lax.rem(y - dy + ys, ys) * 2 + core
         return remote(
-            rows.at[h, held, src], rows.at[h, held, src], sc3, rc3.at[h], {"tp": q}
+            rows.at[h, held, src], rows.at[h, held, src], sc3, rc3.at[h, away if h == HALVES - 1 and nz % 2 == 0 else 0], {"tp": q}
         )
 
     def copy_g(dy, h):
@@ -405,7 +405,7 @@
     near = [peer_of(z, dx) for dx in range(1, nx)]
     near = near + [peer_of(across(j), dx) for j in range(ncross, nz - 1) for dx in range(nx)]
 
-    for h in range(HALVES):
+    def reduce_half(h):
         copy_d1(y, h).wait_recv()
         total = tokens[:, block(t, h)].astype(F32) + op_o[y, h] + op_r[y, h].astype(F32)
         for dy in range(1, ys):
@@ -417,6 +417,7 @@
             copy_g(dy, h).start()
         sd[h] = dot(dispatch, mb[h]).reshape(n, cap, sw).astype(BF16)
 
+    def send_half(h):
         @pl.loop(0, ncross)
         def _(j):
             for dx in range(nx):
@@ -427,47 +428,65 @@
         rows[h, t, e] = sd[h, e]
         copy_c3(0, e, h).start()
 
+    reduce_half(0)
+    send_half(0)
+    reduce_half(1)
+
     gs = min(n, max(1, 64 // cap))
     span = gs * cap
     hidden = hid.shape[1]
     fc = min(256, hidden)
 
-    def scaled_rows(h):
-        mate = rows.at[h, pl.ds(0, ys)]
-        remote(mate, mate, sc3, rc3.at[h], {"tp": q}).wait_recv()
-
-        @pl.loop(0, n // gs)
+    split = 2 if nz % 2 == 0 else 1
+    count = n // split
+
+    def scaled_rows(h, first, number, away):
+        mate = rows.at[h, pl.ds(0, ys), pl.ds(0, number)]
+        remote(mate, mate, sc3, rc3.at[h, away], {"tp": q}).wait_recv()
+
+        @pl.loop(0, number // gs)
         def _(g):
-            at = pl.ds(pl.multiple_of(g * span, span), span)
+            at = pl.ds(pl.multiple_of(first * cap + g * span, span), span)
             acc = jnp.zeros((span, 1), F32)
             for i in range(p):
                 lo = i * share + h * sw
-                v = rows[h, i, pl.ds(g * gs, gs)].astype(F32).reshape(span, sw)
+                v = rows[h, i, pl.ds(first + g * gs, gs)].astype(F32).reshape(span, sw)
                 acc = acc + jnp.sum(v * v, axis=1, keepdims=True)
                 xn[h, at, i * sw:(i + 1) * sw] = (v * moe_gain[:, lo:lo + sw]).astype(BF16)
             ssq[at, :] = acc if h == 0 else ssq[at, :] + acc
 
-    def partial_dot(weight, h, cs):
+    def rows_at(first, number):
+        return pl.ds(pl.multiple_of(first * cap, count * cap), number * cap)
+
+    def partial_dot(weight, h, at, cs):
         acc = None
         for i in range(p):
             lo = i * share + h * sw
-            piece = dot(xn[h, :, i * sw:(i + 1) * sw], weight[lo:lo + sw, cs])
+            piece = dot(xn[h, at, i * sw:(i + 1) * sw], weight[lo:lo + sw, cs])
             acc = piece if acc is None else acc + piece
         return acc
 
-    def early(k, weight, f):
+    def early(k, weight, f, h, first, number):
         cs = slice(f * fc, (f + 1) * fc)
-        gacc[k, :, cs] = partial_dot(weight, 0, cs)
-
-    def first_half():
-        loads[5].wait()
-        loads[6].wait()
-        scaled_rows(0)
-
-    tasks = [first_half]
-    for f in range(hidden // fc):
-        tasks.append(functools.partial(early, 0, weg, f))
-        tasks.append(functools.partial(early, 1, weu, f))
+        at = rows_at(first, number)
+        value = partial_dot(weight, h, at, cs)
+        gacc[k, at, cs] = value if h == 0 else gacc[k, at, cs] + value
+
+    def dots(h, first, number):
+        for f in range(hidden // fc):
+            early(0, weg, f, h, first, number)
+            early(1, weu, f, h, first, number)
+
+    def activate(first, number):
+        at = rows_at(first, number)
+        row_scale = lax.rsqrt(ssq[at, :] / width + 1e-06)
+        for f in range(hidden // fc):
+            cs = slice(f * fc, (f + 1) * fc)
+            gate_part = gacc[0, at, cs] * row_scale
+            hid[at, cs] = (jax.nn.silu(gate_part) * (gacc[1, at, cs] * row_scale)).astype(BF16)
+
+    here = high * count if split == 2 else 0
+    there = (1 - high) * count if split == 2 else 0
 
     def gathered(h):
         for dy in range(1, ys):
@@ -491,54 +510,48 @@
     def pass_on(src, h):
         for dy in range(1, ys):
             landed_c2(dy, src, h).wait_recv()
-            copy_c3(dy, src, h).start()
+            copy_c3(dy, src, h, 1).start()
 
     def cross(src, h):
         landed_c1(src, h).wait_recv()
         for dy in range(1, ys):
             copy_c2(dy, src, h).start()
-        copy_c3(0, src, h).start()
-
+        copy_c3(0, src, h, 1).start()
+
+    def each(action, sources, h):
+        for src in sources:
+            action(src, h)
+
+    nearest = beyond[0] if beyond else []
+    farthest = [src for group in beyond[1:] for src in group]
     gathered(0)
-    for h in range(HALVES):
-        for i, group in enumerate(beyond):
-            for src in group:
-                cross(src, h)
-            if h == 0 and i == 0:
-                gathered(1)
-            if h and i == 0:
-                for src in near:
-                    near_own(src, 0)
-                    near_other(src, 0)
-        if h == 0:
-            for group in beyond[:-1]:
-                for src in group:
-                    pass_on(src, 0)
-    for src in beyond[-1] if beyond else []:
-        pass_on(src, 0)
-    if not beyond:
-        gathered(1)
-        for src in near:
-            near_own(src, 0)
-            near_other(src, 0)
-    rest = [functools.partial(near_own, src, 1) for src in near]
-    rest = rest + [functools.partial(near_other, src, 1) for src in near]
-    for step in rest:
-        step()
-    rest = [functools.partial(pass_on, src, 1) for group in beyond for src in group]
-    while rest:
-        tasks.pop(0)() if tasks else None
-        rest.pop(0)()
-    for task in tasks:
-        task()
-
-    scaled_rows(HALVES - 1)
-    row_scale = lax.rsqrt(ssq[...] / width + 1e-06)
-    for f in range(hidden // fc):
-        cs = slice(f * fc, (f + 1) * fc)
-        gate_part = (gacc[0, :, cs] + partial_dot(weg, 1, cs)) * row_scale
-        up_part = (gacc[1, :, cs] + partial_dot(weu, 1, cs)) * row_scale
-        hid[:, cs] = (jax.nn.silu(gate_part) * up_part).astype(BF16)
+    send_half(1)
+    each(cross, farthest, 0)
+    gathered(1)
+    each(cross, nearest, 0)
+    each(pass_on, farthest, 0)
+    each(near_own, near, 0)
+    each(near_other, near, 0)
+    each(pass_on, nearest, 0)
+    each(cross, farthest, 1)
+    each(cross, nearest, 1)
+    each(near_own, near, 1)
+    each(near_other, near, 1)
+    loads[5].wait()
+    loads[6].wait()
+    scaled_rows(0, 0, n, 0)
+    dots(0, 0, n)
+    each(pass_on, farthest, 1)
+    each(pass_on, nearest, 1)
+    if split == 2:
+        scaled_rows(HALVES - 1, here, count, 0)
+        dots(HALVES - 1, here, count)
+
+    scaled_rows(HALVES - 1, there, count, split - 1)
+    dots(HALVES - 1, there, count)
+    activate(there, count)
+    if split == 2:
+        activate(here, count)
 
     loads[7].wait()
     chunk = nx * cap
@@ -742,7 +755,7 @@
         dma, dma((nz, nx - 1, nc)), dma, dma((nz + 1, nc)), dma, dma((nx - 1, nc - nc // 2)),
         dma, dma((ys, nh)), dma, dma((ys - 1, nh)),
         dma, dma((ys - 1, nh)), dma,
-        dma, dma((n, nh)), dma, dma((ys - 1, n, nh)), dma, dma((nh,)),
+        dma, dma((n, nh)), dma, dma((ys - 1, n, nh)), dma, dma((nh, 2)),
         dma, dma((nz, ys, nh)), dma, dma((nz, ys - 1, nh)), dma((ys - 1, nx, nh)), dma, dma((nh,)),
     ]
     outs = (

time: 84.2 us -> 81.3 us (0.966)
  Pallas kernels: 83.4 us -> 80.5 us
    pallas_call x1, Pallas kernels: 81.3 us -> 78.5 us  [shards(): pl.pallas_call(functools.partial(kernel, n, p, nx, cap), out_shape=outs,...]
where the time goes in v6:
time: 81.3 us; the launch traced here: 81.1 us
  Pallas kernels  80.5 us (99%)
    pallas_call x1, Pallas kernels, shards(): pl.pallas_call(functools.partial(kernel, n, p, nx, cap), out_shape=outs,...  78.5 us
    pallas_call x1, Pallas kernels, shards(): pl.pallas_call(finish, out_shape=outs, in_specs=[vm] * 3, out_specs=(vm,...  2.03 us

profile of v6, /device:TPU:0, one launch (start us, length us, event | category | flops | bytes accessed | tf_op | source)
XLA Modules:
  0.0 81.1 jit_solution(1766507910050776753)
XLA Ops:
  0.6 78.5 %shard_map.184 = (bf16[64,1024]{1,0:T(8,128)(2,1)}, f32[64,1024]{1,0:T(8,128)}, bf16[3,64,1024]{2,1,0:T(8,128)(2,1)}) custom-call(bf16[64,4096]{1,0:T(8,128)(2,1)} %tokens_h.1, f32[64,1024]{1,0:T(8,128)} %state_h.1, bf16[3,64,1024]{2,1,0:T(8,128)(2,1)} %bitcast.7, bf16[32,128]{1,0:T(8,128)(2,1)} %bitcast.8, bf16[32,128]{1,0:T(8,128)(2,1)} %bitcast.9, ...), custom_call_target="tpu_custom_call" | custom-call | tf_op jit(solution)/shard_map/pallas_call | solution.py:766
  79.1 2.0 %shard_map.185 = (bf16[64,1024]{1,0:T(8,128)(2,1)}, f32[64,1024]{1,0:T(8,128)}, bf16[3,64,1024]{2,1,0:T(8,128)(2,1)}) custom-call(bf16[64,1024]{1,0:T(8,128)(2,1)} %get-tuple-element.9.layer_in, f32[64,1024]{1,0:T(8,128)} %get-tuple-element.10.state_in, bf16[3,64,1024]{2,1,0:T(8,128)(2,1)} %get-tuple-element.11.conv_in), custom_call_target="tpu_custom_call" | custom-call | tf_op jit(solution)/shard_map/pallas_call | solution.py:779

commit v7 on v6

--- a/solution.py
+++ b/solution.py
@@ -80,9 +80,6 @@
     def _(d):
         pl.semaphore_signal(barrier, inc=1, device_id={"tp": lax.rem(t + d, p)}, device_id_type=MESH)
 
-    for load in small[2:] + loads[:4]:
-        load.start()
-
     @pl.when(z == 0)
     def _():
         rz[0] = jnp.zeros(rz.shape[1:], BF16)
@@ -93,6 +90,8 @@
 
     small[0].wait()
     small[1].wait()
+    for load in loads[:2] + small[2:] + loads[2:4]:
+        load.start()
     nc, bw = rate_h.shape[0], rate_h.shape[1]
     late = nc // 2
     paired = nz % 2 == 0 and nz > 2
@@ -550,8 +549,6 @@
     scaled_rows(HALVES - 1, there, count, split - 1)
     dots(HALVES - 1, there, count)
     activate(there, count)
-    if split == 2:
-        activate(here, count)
 
     loads[7].wait()
     chunk = nx * cap
@@ -642,7 +639,11 @@
 
     order = [across(j) for j in range(nz - 1)] + [z]
     pairs = [order[i:i + 2] for i in range(0, nz, 2)]
-    for planes in pairs:
+    waiting = split == 2
+    for i, planes in enumerate(pairs):
+        if waiting and 2 * i + len(planes) > ncross:
+            waiting = False
+            activate(here, count)
         issue(planes, range(1, ys))
         issue(planes, [0])
         for plane in planes:

time: 81.3 us -> 81.2 us (level)
  no operation moved by 1% of the time
where the time goes in v7:
time: 81.2 us; the launch traced here: 81.1 us
  Pallas kernels  80.4 us (99%)
    pallas_call x1, Pallas kernels, shards(): pl.pallas_call(functools.partial(kernel, n, p, nx, cap), out_shape=outs,...  78.4 us
    pallas_call x1, Pallas kernels, shards(): pl.pallas_call(finish, out_shape=outs, in_specs=[vm] * 3, out_specs=(vm,...  2.03 us

profile of v7, /device:TPU:0, one launch (start us, length us, event | category | flops | bytes accessed | tf_op | source)
XLA Modules:
  0.0 81.1 jit_solution(17884790946933051798)
XLA Ops:
  0.6 78.4 %shard_map.184 = (bf16[64,1024]{1,0:T(8,128)(2,1)}, f32[64,1024]{1,0:T(8,128)}, bf16[3,64,1024]{2,1,0:T(8,128)(2,1)}) custom-call(bf16[64,4096]{1,0:T(8,128)(2,1)} %tokens_h.1, f32[64,1024]{1,0:T(8,128)} %state_h.1, bf16[3,64,1024]{2,1,0:T(8,128)(2,1)} %bitcast.7, bf16[32,128]{1,0:T(8,128)(2,1)} %bitcast.8, bf16[32,128]{1,0:T(8,128)(2,1)} %bitcast.9, ...), custom_call_target="tpu_custom_call" | custom-call | tf_op jit(solution)/shard_map/pallas_call | solution.py:767
  79.1 2.0 %shard_map.185 = (bf16[64,1024]{1,0:T(8,128)(2,1)}, f32[64,1024]{1,0:T(8,128)}, bf16[3,64,1024]{2,1,0:T(8,128)(2,1)}) custom-call(bf16[64,1024]{1,0:T(8,128)(2,1)} %get-tuple-element.9.layer_in, f32[64,1024]{1,0:T(8,128)} %get-tuple-element.10.state_in, bf16[3,64,1024]{2,1,0:T(8,128)(2,1)} %get-tuple-element.11.conv_in), custom_call_target="tpu_custom_call" | custom-call | tf_op jit(solution)/shard_map/pallas_call | solution.py:780
